TPU v7x, 512 devices: a whole 4x8x8 slice. The times are simulated.
512 devices in a mesh: ep: 32 (over z, x), tp: 16 (over y, core).
Axes of the slice: x: 4, y: 8, z: 8, core: 2. Of those that a mesh axis runs over, the one named last changes fastest.
Arguments:
- mixer_in: bfloat16 [4096, 2048], P('ep'), may hold values from -6 to 6
- mixer_gain: float32 [2048], replicated, may hold values from 0.1 to 1.9
- w_value: bfloat16 [2048, 1536], P(None, 'tp'), may hold values from -0.125 to 0.125
- w_gate: bfloat16 [2048, 1536], P(None, 'tp'), may hold values from -0.125 to 0.125
- w_taps: float32 [31, 1536], P(None, 'tp'), may hold values from -3 to 3
- channel_gain: float32 [1536], P('tp'), may hold values from 0.1 to 1.9
- w_output: bfloat16 [1536, 2048], P('tp'), may hold values from -0.15625 to 0.15625
- expert_in: bfloat16 [4096, 2048], P('ep'), may hold values from -6 to 6
- expert_gain: float32 [2048], replicated, may hold values from 0 to 8
- route_experts: int32 [4096, 4], P('ep'), may hold values from 0 to 31, all different within a row; in each aligned block of 128 rows (0 to 127, 128 to 255, ...) at most 32 rows name the same one
- route_scores: float32 [4096, 4], P('ep'), may hold values from -6 to 6
- expert_gate: bfloat16 [32, 2048, 2048], P('ep', None, 'tp'), may hold values from -0.125 to 0.125
- expert_up: bfloat16 [32, 2048, 2048], P('ep', None, 'tp'), may hold values from -0.125 to 0.125
- expert_down: bfloat16 [32, 2048, 2048], P('ep', 'tp'), may hold values from -0.125 to 0.125
Outputs:
- mixer_out: bfloat16 [4096, 2048], P('ep')
- expert_out: bfloat16 [4096, 2048], P('ep')
Inputs may be any that keep to these rules, and one draw needn't show every extreme that they name: `route_experts`: each row names 4 different experts. In each aligned block of 128 rows (the rows of one index of ep) no expert is named more than 32 times, a bound that some block reaches.
All inputs are finite; a program needn't handle non-finite values.
Results may differ from a plain program's by a relative error of at most 0.02.
Values may be sent and summed in bfloat16 or wider, within the bound.
No kernel may reach another device: no remote copies, remote signals or barrier semaphores. Data moves between devices by JAX's collectives and lax.ppermute only.
A program may use at most 64 MiB of HBM per device.

v0:
```python
import jax
import jax.numpy as jnp
from jax import lax
from jax.experimental import pallas as pl
from jax.experimental.pallas import tpu as pltpu
from jax.sharding import Mesh
from jax.sharding import PartitionSpec as P

CONV_CH = 1536
CONV_W = 31
TOP_K = 4
BITS = ("y2", "y1", "y0", "c")
TP = BITS
Y = BITS[:3]
GROUP = 4
EXPERTS = 32


epsilon = 1e-05
clamp_limit = 7.0
swish_slope = 1.702


def shifted(block, axis, distance):
    devices = range(lax.axis_size(axis))
    route = [(i - distance, i) for i in devices if i - distance in devices]
    return lax.ppermute(block, axis, route)


def swapped(x, axis):
    return lax.ppermute(x, axis, [(0, 1), (1, 0)])


def exchanged(x, axis):
    return lax.all_to_all(x, axis, split_axis=0, concat_axis=0, tiled=True)


def core_half(x):
    rows, width = x.shape
    x = x.reshape(2, rows // 2, width)
    own = lax.axis_index("c")
    kept = lax.dynamic_index_in_dim(x, own, 0, keepdims=False)
    given = lax.dynamic_index_in_dim(x, 1 - own, 0, keepdims=False)
    return kept + swapped(given.astype(jnp.bfloat16), "c").astype(jnp.float32)


def totals(halves):
    size = lax.axis_size(Y)
    rows, width = halves[0].shape
    share = rows // size
    parts = [half.astype(jnp.bfloat16).reshape(size, 1, share, width) for half in halves]
    arrived = exchanged(jnp.concatenate(parts, axis=1), Y)
    summed = jnp.sum(arrived.astype(jnp.float32), axis=0).astype(jnp.bfloat16)
    gathered = exchanged(jnp.broadcast_to(summed, (size, *summed.shape)), Y)
    others = swapped(gathered, "c")
    return placed(gathered, others)


def row_norm(inputs, gains):
    widened = inputs.astype(jnp.float32)
    row_mean = jnp.mean(widened, axis=-1, keepdims=True)
    row_var = jnp.mean(jnp.square(widened - row_mean), axis=-1, keepdims=True)
    return (widened - row_mean) * lax.rsqrt(row_var + epsilon) * gains


def convolved(mixer_in, mixer_gain, w_value, w_gate, w_taps):
    normed = row_norm(mixer_in, mixer_gain).astype(jnp.bfloat16)
    values = jnp.dot(normed, w_value, preferred_element_type=jnp.float32)
    gate_pre = jnp.dot(normed, w_gate, preferred_element_type=jnp.float32)
    gated_values = (values * jax.nn.sigmoid(gate_pre)).astype(jnp.bfloat16)
    mixer_rows = gated_values.shape[0]
    reach_rows = CONV_W - 1
    earlier = shifted(gated_values[mixer_rows - reach_rows :], "ep", 1)
    extended = jnp.concatenate([earlier, gated_values], axis=0)
    conv_out = jnp.zeros(gated_values.shape, jnp.float32)
    for offset in range(CONV_W):
        conv_out = (
            conv_out + extended[offset : offset + mixer_rows].astype(jnp.float32) * w_taps[offset]
        )
    return conv_out


def projected(conv_out, channel_gain, w_output):
    sums = jnp.stack([jnp.sum(conv_out, axis=1), jnp.sum(conv_out * conv_out, axis=1)])
    everyone = lax.all_gather(sums, TP)
    sums = jnp.sum(everyone, axis=0)
    row_mean = (sums[0] / CONV_CH)[:, None]
    row_var = (sums[1] / CONV_CH)[:, None] - row_mean * row_mean
    activated = jax.nn.silu(
        (conv_out - row_mean) * lax.rsqrt(row_var + epsilon) * channel_gain
    ).astype(jnp.bfloat16)
    return jnp.dot(activated, w_output, preferred_element_type=jnp.float32)


def places(ids_ref, rows):
    names = lax.broadcasted_iota(jnp.int32, (EXPERTS, rows), 0)
    named = [ids_ref[pl.ds(k, 1), :] == names for k in range(TOP_K)]
    chosen = jnp.zeros((EXPERTS, rows), jnp.float32)
    for k in range(TOP_K):
        chosen = jnp.where(named[k], 1.0, chosen)
    earlier = lax.broadcasted_iota(jnp.int32, (rows, rows), 0)
    later = lax.broadcasted_iota(jnp.int32, (rows, rows), 1)
    before = jnp.where(earlier < later, 1.0, 0.0).astype(jnp.bfloat16)
    rank = jnp.dot(chosen.astype(jnp.bfloat16), before, preferred_element_type=jnp.float32)
    return named, jnp.where(chosen > 0.0, rank, -1.0).astype(jnp.bfloat16)


def spread_over(sent, per_expert):
    of_row = lax.broadcasted_iota(jnp.int32, (sent, EXPERTS), 0) // per_expert
    of_col = lax.broadcasted_iota(jnp.int32, (sent, EXPERTS), 1)
    return jnp.where(of_row == of_col, 1.0, 0.0).astype(jnp.bfloat16)


def taken_by(place, spread, slots, member):
    sent, rows = spread.shape[0], place.shape[1]
    slot = lax.broadcasted_iota(jnp.int32, (sent, rows), 0) % slots * GROUP + member
    return jnp.dot(spread, place, preferred_element_type=jnp.float32) == slot.astype(jnp.float32)


def front_kernel(member, x_ref, gain_ref, ids_ref, rows_ref):
    rows = x_ref.shape[0]
    sent = rows_ref.shape[0]
    slots = sent // EXPERTS
    normed = row_norm(x_ref[...], gain_ref[...]).astype(jnp.bfloat16)
    _, place = places(ids_ref, rows)
    taken = taken_by(place, spread_over(sent, slots), slots, member[0])
    select = jnp.where(taken, 1.0, 0.0).astype(jnp.bfloat16)
    rows_ref[...] = jnp.dot(select, normed, preferred_element_type=jnp.float32).astype(jnp.bfloat16)


def front(member, x, gain, ids, sent):
    _, width = x.shape
    whole = pl.BlockSpec(memory_space=pltpu.VMEM)
    return pl.pallas_call(
        front_kernel,
        in_specs=[pl.BlockSpec(memory_space=pltpu.SMEM)] + [whole] * 3,
        out_specs=whole,
        out_shape=jax.ShapeDtypeStruct((sent, width), jnp.bfloat16),
        compiler_params=pltpu.CompilerParams(vmem_limit_bytes=57000 << 10),
        name="front",
    )(member.reshape(1), x, gain.reshape(1, width), ids)


def mixing_kernel(member, ids_ref, scores_ref, hi_ref, lo_ref):
    sent, rows = hi_ref.shape
    slots = sent // EXPERTS
    raised = [jnp.exp(scores_ref[pl.ds(k, 1), :]) for k in range(TOP_K)]
    total = raised[0] + raised[1] + raised[2] + raised[3]
    named, place = places(ids_ref, rows)
    weights = jnp.zeros((EXPERTS, rows), jnp.float32)
    for k in range(TOP_K):
        weights = jnp.where(named[k], raised[k] / total, weights)
    weights_hi = weights.astype(jnp.bfloat16)
    weights_lo = (weights - weights_hi.astype(jnp.float32)).astype(jnp.bfloat16)
    spread = spread_over(sent, slots)
    taken = taken_by(place, spread, slots, member[0])
    wide_hi = jnp.dot(spread, weights_hi, preferred_element_type=jnp.float32)
    wide_lo = jnp.dot(spread, weights_lo, preferred_element_type=jnp.float32)
    hi_ref[...] = jnp.where(taken, wide_hi, 0.0).astype(jnp.bfloat16)
    lo_ref[...] = jnp.where(taken, wide_lo, 0.0).astype(jnp.bfloat16)


def mixing(member, ids, scores, sent):
    rows = ids.shape[1]
    whole = pl.BlockSpec(memory_space=pltpu.VMEM)
    return pl.pallas_call(
        mixing_kernel,
        in_specs=[pl.BlockSpec(memory_space=pltpu.SMEM)] + [whole] * 2,
        out_specs=[whole] * 2,
        out_shape=[jax.ShapeDtypeStruct((sent, rows), jnp.bfloat16)] * 2,
        compiler_params=pltpu.CompilerParams(vmem_limit_bytes=4 << 20),
        name="mixing",
    )(member.reshape(1), ids, scores)


def hidden_kernel(x_ref, *refs):
    gus, out_ref = refs[:GROUP], refs[GROUP]
    inner = gus[0].shape[1] // 2
    for at, gu in enumerate(gus):
        both = jnp.dot(x_ref[...], gu[...], preferred_element_type=jnp.float32)
        g = jnp.minimum(both[:, :inner], clamp_limit)
        u = jnp.clip(both[:, inner:], -clamp_limit, clamp_limit)
        hidden = (u + 1.0) * g * jax.nn.sigmoid(swish_slope * g)
        out_ref[:, at * inner : (at + 1) * inner] = hidden.astype(jnp.bfloat16)


def down_kernel(hidden_ref, *refs):
    downs, out_hbm, out_buf, sems = refs[:GROUP], refs[GROUP], refs[GROUP + 1], refs[GROUP + 2]
    parts = sems.shape[0]
    step = out_hbm.shape[1] // parts
    copies = []
    for part in range(parts):
        own = pl.ds(part * step, step)
        weights = jnp.concatenate([down[:, own] for down in downs], axis=0)
        out_buf[:, own] = jnp.dot(
            hidden_ref[...], weights, preferred_element_type=jnp.float32
        ).astype(jnp.bfloat16)
        copies.append(pltpu.make_async_copy(out_buf.at[:, own], out_hbm.at[:, own], sems.at[part]))
        copies[-1].start()
    for copy in copies:
        copy.wait()


WHOLE = pl.BlockSpec(memory_space=pltpu.VMEM)
OUTSIDE = pl.BlockSpec(memory_space=pl.ANY)


def hidden_units(x, gus):
    units = GROUP * gus[0].shape[1] // 2
    return pl.pallas_call(
        hidden_kernel,
        in_specs=[WHOLE] * (1 + GROUP),
        out_specs=WHOLE,
        out_shape=jax.ShapeDtypeStruct((x.shape[0], units), jnp.bfloat16),
        compiler_params=pltpu.CompilerParams(vmem_limit_bytes=53000 << 10),
        name="hidden",
    )(x, *gus)


def projected_down(hidden, downs):
    shape = (hidden.shape[0], downs[0].shape[1])
    return pl.pallas_call(
        down_kernel,
        in_specs=[WHOLE] * (1 + GROUP),
        out_specs=OUTSIDE,
        out_shape=jax.ShapeDtypeStruct(shape, jnp.bfloat16),
        scratch_shapes=[pltpu.VMEM(shape, jnp.bfloat16), pltpu.SemaphoreType.DMA((4,))],
        compiler_params=pltpu.CompilerParams(vmem_limit_bytes=53000 << 10),
        name="project",
    )(hidden, *downs)


def placing_kernel(core, own_ref, other_ref, *refs):
    outs, sems = refs[:-1], refs[-1]
    copies = []
    for at, out in enumerate(outs):
        for side, ref in enumerate((own_ref, other_ref)):
            place = core[0] if side == 0 else 1 - core[0]
            copies.append(pltpu.make_async_copy(ref.at[:, at], out.at[place], sems.at[at, side]))
            copies[-1].start()
    for copy in copies:
        copy.wait()


def placed(own, other):
    blocks, count, rows, width = own.shape
    core = lax.axis_index("c").astype(jnp.int32).reshape(1)
    outs = pl.pallas_call(
        placing_kernel,
        in_specs=[pl.BlockSpec(memory_space=pltpu.SMEM), OUTSIDE, OUTSIDE],
        out_specs=[OUTSIDE] * count,
        out_shape=[jax.ShapeDtypeStruct((2, blocks, rows, width), own.dtype)] * count,
        scratch_shapes=[pltpu.SemaphoreType.DMA((count, 2))],
        compiler_params=pltpu.CompilerParams(vmem_limit_bytes=1 << 20),
        name="placing",
    )(core, own, other)
    return [out.reshape(2 * blocks * rows, width) for out in outs]


def program(
    mixer_in,
    mixer_gain,
    w_value,
    w_gate,
    w_taps,
    channel_gain,
    w_output,
    expert_in,
    expert_gain,
    route_experts,
    route_scores,
    expert_gate,
    expert_up,
    expert_down,
):
    rows_b, width = expert_in.shape
    experts = lax.axis_size("ep")
    capacity = 2 * rows_b * TOP_K // experts
    slots = capacity // GROUP
    member = lax.axis_index(("y0", "c")).astype(jnp.int32)

    gate_up = jnp.concatenate([expert_gate[0], expert_up[0]], axis=1)
    down = expert_down[0]
    gu_y = swapped(gate_up, "y0")
    down_y = swapped(down, "y0")
    gu_c = swapped(gate_up, "c")
    down_c = swapped(down, "c")
    gu_d = swapped(gu_y, "c")
    down_d = swapped(down_y, "c")

    ids = route_experts.T
    sending = front(member, expert_in, expert_gain, ids, experts * slots)
    arrived = exchanged(sending.reshape(experts, slots, width), "ep").reshape(-1, width)

    mixing_hi, mixing_lo = mixing(member, ids, route_scores.T, experts * slots)
    conv_out = convolved(mixer_in, mixer_gain, w_value, w_gate, w_taps)
    mixer_partial = projected(conv_out, channel_gain, w_output)
    mixer_half = core_half(mixer_partial)

    hidden = hidden_units(arrived, (gate_up, gu_c, gu_y, gu_d))
    partial = projected_down(hidden, (down, down_c, down_y, down_d))
    returned = exchanged(partial.reshape(experts, slots, width), "ep").reshape(-1, width)

    def mixed(m):
        return lax.dot_general(
            m, returned, (((0,), (0,)), ((), ())), preferred_element_type=jnp.float32
        )

    expert_half = core_half(mixed(mixing_hi) + mixed(mixing_lo))
    mixer_out, expert_out = totals([mixer_half, expert_half])
    return (mixer_out, expert_out)


def solution(mesh):
    split = Mesh(mesh.devices.reshape(mesh.shape["ep"], 2, 2, 2, 2), ("ep", *TP))
    in_specs = (
        P("ep", None),
        P(),
        P(None, TP),
        P(None, TP),
        P(None, TP),
        P(TP),
        P(TP, None),
        P("ep", None),
        P(),
        P("ep", None),
        P("ep", None),
        P("ep", None, TP),
        P("ep", None, TP),
        P("ep", TP, None),
    )
    out_specs = (P("ep", None), P("ep", None))
    return jax.shard_map(program, mesh=split, in_specs=in_specs, out_specs=out_specs, check_vma=False)
```

profile of v0, /device:TPU:65, one launch (start us, length us, event | category | flops | bytes accessed | tf_op | source)
XLA Modules:
  0.0 160.0 jit_solution(15485883641184342808)
XLA Ops:
  0.6 0.0 copy-start
  0.6 2.3 %pad_maximum_fusion.refs_0_ = bf16[2048,256]{1,0:T(8,128)(2,1)} fusion(bf16[2048,128]{1,0:T(8,128)(2,1)} %bitcast.134, bf16[2048,128]{1,0:T(8,128)(2,1)} %bitcast.135), kind=kLoop, calls=%fused_computation.14 | loop fusion | flops 2097152 | bytes 2097152 | tf_op jit(solution)/shard_map/concatenate | solution.py:282
  3.0 3.2 %collective-permute-start.3 = (bf16[2048,256]{1,0:T(8,128)(2,1)}, bf16[2048,256]{1,0:T(8,128)(2,1)}, u32[]{:S(2)}, u32[]{:S(2)}) collective-permute-start(bf16[2048,256]{1,0:T(8,128)(2,1)} %pad_maximum_fusion.refs_0_), channel_id=1, source_target_pairs={{0,2},{2,0},{1,3},{3,1},{4,6},{6,4},{5,7},{7,5},{8,10},{10,8},{9,1... | collective-permute-start | bytes 3145736 | tf_op jit(solution)/shard_map/ppermute | solution.py:31
  6.2 2.8 %front.1 = bf16[256,2048]{1,0:T(8,128)(2,1)} custom-call(s32[1]{0:T(128)} %bitcast.41.member, bf16[128,2048]{1,0:T(8,128)(2,1)} %x_ref.1, f32[1,2048]{1,0:T(1,128)} %bitcast.136, s32[4,128]{1,0:T(4,128)} %bitcast.125), custom_call_target="tpu_custom_call" | custom-call | tf_op jit(solution)/shard_map/front/pallas_call | solution.py:134
  9.0 12.2 %all-to-all-start = ((bf16[32,8,2048]{2,1,0:T(8,128)(2,1)}), bf16[32,8,2048]{2,1,0:T(8,128)(2,1)S(1)}, u32[]{:S(2)}, u32[]{:S(2)}) async-start(bf16[32,8,2048]{2,1,0:T(8,128)(2,1)} %bitcast.129), calls=%async_computation | async-start | bytes 2097152 | tf_op jit(solution)/shard_map/all_to_all | solution.py:35
  21.2 2.1 %collective-permute-start.6 = (bf16[128,2048]{1,0:T(8,128)(2,1)S(1)}, bf16[128,2048]{1,0:T(8,128)(2,1)S(1)}, u32[]{:S(2)}, u32[]{:S(2)}) collective-permute-start(bf16[128,2048]{1,0:T(8,128)(2,1)S(1)} %bitcast.122), channel_id=1, source_target_pairs={{0,2},{2,0},{1,3},{3,1},{4,6},{6,4},{5,7},{7,5},{8,10},{10,8},{9,1... | collective-permute-start | bytes 1572872 | tf_op jit(solution)/shard_map/ppermute | solution.py:31
  23.3 3.7 %collective-permute-start.2 = (bf16[2048,256]{1,0:T(8,128)(2,1)}, bf16[2048,256]{1,0:T(8,128)(2,1)}, u32[]{:S(2)}, u32[]{:S(2)}) collective-permute-start(bf16[2048,256]{1,0:T(8,128)(2,1)} %pad_maximum_fusion.refs_0_), channel_id=1, source_target_pairs={{0,1},{1,0},{2,3},{3,2},{4,5},{5,4},{6,7},{7,6},{8,9},{9,8},{10,11... | collective-permute-start | bytes 3145736 | tf_op jit(solution)/shard_map/ppermute | solution.py:31
  27.0 2.2 %collective-permute-done.3.refs_2_ = bf16[2048,256]{1,0:T(8,128)(2,1)} collective-permute-done((bf16[2048,256]{1,0:T(8,128)(2,1)}, bf16[2048,256]{1,0:T(8,128)(2,1)}, u32[]{:S(2)}, u32[]{:S(2)}) %collective-permute-start.3) | collective-permute-done | bytes 1048608 | tf_op jit(solution)/shard_map/ppermute | solution.py:31
  29.2 4.6 %collective-permute-start.4 = (bf16[2048,256]{1,0:T(8,128)(2,1)}, bf16[2048,256]{1,0:T(8,128)(2,1)}, u32[]{:S(2)}, u32[]{:S(2)}) collective-permute-start(bf16[2048,256]{1,0:T(8,128)(2,1)} %collective-permute-done.3.refs_2_), channel_id=1, source_target_pairs={{0,1},{1,0},{2,3},{3,2},{4,5},{5,4},{6,7},{7,6},{8,9},{9,8},{10,11... | collective-permute-start | bytes 3145736 | tf_op jit(solution)/shard_map/ppermute | solution.py:31
  33.8 1.9 %collective-permute-start.5 = (bf16[128,2048]{1,0:T(8,128)(2,1)S(1)}, bf16[128,2048]{1,0:T(8,128)(2,1)S(1)}, u32[]{:S(2)}, u32[]{:S(2)}) collective-permute-start(bf16[128,2048]{1,0:T(8,128)(2,1)S(1)} %bitcast.123), channel_id=1, source_target_pairs={{0,1},{1,0},{2,3},{3,2},{4,5},{5,4},{6,7},{7,6},{8,9},{9,8},{10,11... | collective-permute-start | bytes 1572872 | tf_op jit(solution)/shard_map/ppermute | solution.py:31
  35.7 0.2 convert_reduce_fusion
  35.9 4.5 %collective-permute-done.6.refs_2_ = bf16[128,2048]{1,0:T(8,128)(2,1)S(1)} collective-permute-done((bf16[128,2048]{1,0:T(8,128)(2,1)S(1)}, bf16[128,2048]{1,0:T(8,128)(2,1)S(1)}, u32[]{:S(2)}, u32[]{:S(2)}) %collective-permute-start.6) | collective-permute-done | bytes 524320 | tf_op jit(solution)/shard_map/ppermute | solution.py:31
  40.4 3.4 %collective-permute-start.7 = (bf16[128,2048]{1,0:T(8,128)(2,1)S(1)}, bf16[128,2048]{1,0:T(8,128)(2,1)}, u32[]{:S(2)}, u32[]{:S(2)}) collective-permute-start(bf16[128,2048]{1,0:T(8,128)(2,1)S(1)} %collective-permute-done.6.refs_2_), channel_id=1, source_target_pairs={{0,1},{1,0},{2,3},{3,2},{4,5},{5,4},{6,7},{7,6},{8,9},{9,8},{10,11... | collective-permute-start | bytes 1572872 | tf_op jit(solution)/shard_map/ppermute | solution.py:31
  43.8 0.3 fusion.7
  44.1 0.0 collective-permute-done.2.refs_1_
  44.1 2.4 %all-to-all-done = bf16[32,8,2048]{2,1,0:T(8,128)(2,1)S(1)} async-done(((bf16[32,8,2048]{2,1,0:T(8,128)(2,1)}), bf16[32,8,2048]{2,1,0:T(8,128)(2,1)S(1)}, u32[]{:S(2)}, u32[]{:S(2)}) %all-to-all-start) | async-done | bytes 1048608 | tf_op jit(solution)/shard_map/all_to_all | solution.py:35
  46.5 0.0 collective-permute-done.4.refs_3_
  46.5 3.5 %hidden.1.hidden_ref = bf16[256,512]{1,0:T(8,128)(2,1)S(1)} custom-call(bf16[256,2048]{1,0:T(8,128)(2,1)S(1)} %bitcast.121, bf16[2048,256]{1,0:T(8,128)(2,1)} %pad_maximum_fusion.refs_0_, bf16[2048,256]{1,0:T(8,128)(2,1)} %collective-permute-done.2.refs_1_, bf16[2048,256]{1,0:T(8,128)(2,1)} %collective-permute-done.3.refs_2_, ...), custom_call_target="tpu_custom_call" | custom-call | tf_op jit(solution)/shard_map/hidden/pallas_call | solution.py:210
  50.0 0.0 collective-permute-done.5.refs_1_
  50.0 2.5 %project.1 = bf16[256,2048]{1,0:T(8,128)(2,1)} custom-call(bf16[256,512]{1,0:T(8,128)(2,1)S(1)} %hidden.1.hidden_ref, bf16[128,2048]{1,0:T(8,128)(2,1)S(1)} %bitcast.124, bf16[128,2048]{1,0:T(8,128)(2,1)S(1)} %collective-permute-done.5.refs_1_, bf16[128,2048]{1,0:T(8,128)(2,1)S(1)} %collective-permute-done.6.refs_2_, ...), custom_call_target="tpu_custom_call" | custom-call | tf_op jit(solution)/shard_map/project/pallas_call | solution.py:222
  52.5 0.0 copy-start.7
  52.6 0.0 copy-start.9
  52.6 9.7 %all-to-all-start.1 = ((bf16[32,8,2048]{2,1,0:T(8,128)(2,1)}), bf16[32,8,2048]{2,1,0:T(8,128)(2,1)S(1)}, u32[]{:S(2)}, u32[]{:S(2)}) async-start(bf16[32,8,2048]{2,1,0:T(8,128)(2,1)} %bitcast.128), calls=%async_computation.1 | async-start | bytes 2097152 | tf_op jit(solution)/shard_map/all_to_all | solution.py:35
  62.3 0.0 copy-start.8
  62.4 0.4 fusion.57
  62.8 0.6 copy-done.8
  63.4 0.4 fusion.6
  63.8 0.1 slice.256
  63.9 3.1 %collective-permute-start = (bf16[30,96]{0,1:T(8,128)(2,1)S(1)}, bf16[30,96]{0,1:T(8,128)(2,1)S(1)}, u32[]{:S(2)}, u32[]{:S(2)}) collective-permute-start(bf16[30,96]{0,1:T(8,128)(2,1)S(1)} %slice.256), channel_id=1, source_target_pairs={{0,16},{16,32},{32,48},{48,64},{64,80},{80,96},{96,112},{112,128},... | collective-permute-start | bytes 17288 | tf_op jit(solution)/shard_map/ppermute | solution.py:27
  67.0 0.3 mixing.1
  67.3 19.8 %collective-permute-done = bf16[30,96]{0,1:T(8,128)(2,1)S(1)} collective-permute-done((bf16[30,96]{0,1:T(8,128)(2,1)S(1)}, bf16[30,96]{0,1:T(8,128)(2,1)S(1)}, u32[]{:S(2)}, u32[]{:S(2)}) %collective-permute-start) | collective-permute-done | bytes 5792 | tf_op jit(solution)/shard_map/ppermute | solution.py:27
  87.1 0.9 fusion.59
  88.0 19.1 %all-gather.1 = f32[16,2,128]{2,1,0:T(2,128)S(1)} all-gather(f32[1,2,128]{2,1,0:T(2,128)S(1)} %maximum_bitcast_fusion), channel_id=2, replica_groups=mesh['ep'=32,'y2'=2,'y1'=2,'y0'=2,'c'=2] {'y2','y1','y0','c'}, dimensions={0}, use_global_device_ids=true | all-gather | bytes 17408 | tf_op jit(solution)/shard_map/all_gather | solution.py:85
  107.2 0.4 fusion.19
  107.6 2.1 %collective-permute-start.1 = (bf16[64,2048]{1,0:T(8,128)(2,1)S(1)}, bf16[64,2048]{1,0:T(8,128)(2,1)S(1)}, u32[]{:S(2)}, u32[]{:S(2)}) collective-permute-start(bf16[64,2048]{1,0:T(8,128)(2,1)S(1)} %fusion.15), channel_id=1, source_target_pairs={{0,1},{1,0},{2,3},{3,2},{4,5},{5,4},{6,7},{7,6},{8,9},{9,8},{10,11... | collective-permute-start | bytes 786440 | tf_op jit(solution)/shard_map/ppermute | solution.py:31
  109.7 0.3 fusion.10
  110.1 0.3 convolution_add_fusion
  110.4 2.2 %collective-permute-start.8 = (bf16[64,2048]{1,0:T(8,128)(2,1)S(1)}, bf16[64,2048]{1,0:T(8,128)(2,1)S(1)}, u32[]{:S(2)}, u32[]{:S(2)}) collective-permute-start(bf16[64,2048]{1,0:T(8,128)(2,1)S(1)} %fusion.16), channel_id=1, source_target_pairs={{0,1},{1,0},{2,3},{3,2},{4,5},{5,4},{6,7},{7,6},{8,9},{9,8},{10,11... | collective-permute-start | bytes 786440 | tf_op jit(solution)/shard_map/ppermute | solution.py:31
  112.7 0.1 fusion.17
  112.8 1.1 collective-permute-done.8
  113.9 0.1 fusion.18
  113.9 0.1 pad_maximum_fusion.1
  114.0 20.6 %all_to_all.20 = bf16[8,2,8,2048]{3,2,1,0:T(8,128)(2,1)S(1)} all-to-all(bf16[8,2,8,2048]{3,2,1,0:T(8,128)(2,1)S(1)} %pad_maximum_fusion.1), channel_id=1, replica_groups=mesh['ep'=32,'y2'=2,'y1'=2,'y0'=2,'c'=2] {'y2','y1','y0'}, dimensions={0} | all-to-all | bytes 1048576 | tf_op jit(solution)/shard_map/all_to_all | solution.py:35
  134.6 0.1 reduce_sum.62
  134.8 17.6 %all_to_all.21.own_ref = bf16[8,2,8,2048]{3,2,1,0:T(8,128)(2,1)S(1)} all-to-all(bf16[8,2,8,2048]{3,2,1,0:T(8,128)(2,1)S(1)} %broadcast_in_dim.2), channel_id=1, replica_groups=mesh['ep'=32,'y2'=2,'y1'=2,'y0'=2,'c'=2] {'y2','y1','y0'}, dimensions={0} | all-to-all | bytes 1048576 | tf_op jit(solution)/shard_map/all_to_all | solution.py:35
  152.4 5.1 %collective-permute-start.9 = (bf16[8,2,8,2048]{3,2,1,0:T(8,128)(2,1)S(1)}, bf16[8,2,8,2048]{3,2,1,0:T(8,128)(2,1)S(1)}, u32[]{:S(2)}, u32[]{:S(2)}) collective-permute-start(bf16[8,2,8,2048]{3,2,1,0:T(8,128)(2,1)S(1)} %all_to_all.21.own_ref), channel_id=1, source_target_pairs={{0,1},{1,0},{2,3},{3,2},{4,5},{5,4},{6,7},{7,6},{8,9},{9,8},{10,11... | collective-permute-start | bytes 1572872 | tf_op jit(solution)/shard_map/ppermute | solution.py:31
  157.5 1.5 collective-permute-done.9.other_ref
  159.0 1.0 placing.1
  (29 shorter events, 0.2 us)
Async XLA Ops:
  0.6 106.5 %copy-start = (bf16[96,2048]{1,0:T(8,128)(2,1)S(1)}, bf16[96,2048]{1,0:T(8,128)(2,1)}, u32[]{:S(2)}) copy-start(bf16[96,2048]{1,0:T(8,128)(2,1)} %param.20) | copy-start | bytes 1179652
  3.0 26.2 %collective-permute-start.3 = (bf16[2048,256]{1,0:T(8,128)(2,1)}, bf16[2048,256]{1,0:T(8,128)(2,1)}, u32[]{:S(2)}, u32[]{:S(2)}) collective-permute-start(bf16[2048,256]{1,0:T(8,128)(2,1)} %pad_maximum_fusion.refs_0_), channel_id=1, source_target_pairs={{0,2},{2,0},{1,3},{3,1},{4,6},{6,4},{5,7},{7,5},{8,10},{10,8},{9,1... | collective-permute-start | bytes 3145736 | tf_op jit(solution)/shard_map/ppermute | solution.py:31
  9.0 12.2 %copy-start.1 = (bf16[1,128,2048]{2,1,0:T(8,128)(2,1)S(1)}, bf16[1,128,2048]{2,1,0:T(8,128)(2,1)}, u32[]{:S(2)}) copy-start(bf16[1,128,2048]{2,1,0:T(8,128)(2,1)} %param.27) | copy-start | bytes 1572868
  9.0 26.7 %copy-start.4 = (bf16[128,2048]{1,0:T(8,128)(2,1)S(1)}, bf16[128,2048]{1,0:T(8,128)(2,1)}, u32[]{:S(2)}) copy-start(bf16[128,2048]{1,0:T(8,128)(2,1)} %param.14) | copy-start | bytes 1572868
  9.0 37.5 %all-to-all-start = ((bf16[32,8,2048]{2,1,0:T(8,128)(2,1)}), bf16[32,8,2048]{2,1,0:T(8,128)(2,1)S(1)}, u32[]{:S(2)}, u32[]{:S(2)}) async-start(bf16[32,8,2048]{2,1,0:T(8,128)(2,1)} %bitcast.129), calls=%async_computation | async-start | bytes 2097152 | tf_op jit(solution)/shard_map/all_to_all | solution.py:35
  21.2 19.1 %collective-permute-start.6 = (bf16[128,2048]{1,0:T(8,128)(2,1)S(1)}, bf16[128,2048]{1,0:T(8,128)(2,1)S(1)}, u32[]{:S(2)}, u32[]{:S(2)}) collective-permute-start(bf16[128,2048]{1,0:T(8,128)(2,1)S(1)} %bitcast.122), channel_id=1, source_target_pairs={{0,2},{2,0},{1,3},{3,1},{4,6},{6,4},{5,7},{7,5},{8,10},{10,8},{9,1... | collective-permute-start | bytes 1572872 | tf_op jit(solution)/shard_map/ppermute | solution.py:31
  23.3 20.8 %collective-permute-start.2 = (bf16[2048,256]{1,0:T(8,128)(2,1)}, bf16[2048,256]{1,0:T(8,128)(2,1)}, u32[]{:S(2)}, u32[]{:S(2)}) collective-permute-start(bf16[2048,256]{1,0:T(8,128)(2,1)} %pad_maximum_fusion.refs_0_), channel_id=1, source_target_pairs={{0,1},{1,0},{2,3},{3,2},{4,5},{5,4},{6,7},{7,6},{8,9},{9,8},{10,11... | collective-permute-start | bytes 3145736 | tf_op jit(solution)/shard_map/ppermute | solution.py:31
  29.2 17.3 %collective-permute-start.4 = (bf16[2048,256]{1,0:T(8,128)(2,1)}, bf16[2048,256]{1,0:T(8,128)(2,1)}, u32[]{:S(2)}, u32[]{:S(2)}) collective-permute-start(bf16[2048,256]{1,0:T(8,128)(2,1)} %collective-permute-done.3.refs_2_), channel_id=1, source_target_pairs={{0,1},{1,0},{2,3},{3,2},{4,5},{5,4},{6,7},{7,6},{8,9},{9,8},{10,11... | collective-permute-start | bytes 3145736 | tf_op jit(solution)/shard_map/ppermute | solution.py:31
  33.8 16.2 %collective-permute-start.5 = (bf16[128,2048]{1,0:T(8,128)(2,1)S(1)}, bf16[128,2048]{1,0:T(8,128)(2,1)S(1)}, u32[]{:S(2)}, u32[]{:S(2)}) collective-permute-start(bf16[128,2048]{1,0:T(8,128)(2,1)S(1)} %bitcast.123), channel_id=1, source_target_pairs={{0,1},{1,0},{2,3},{3,2},{4,5},{5,4},{6,7},{7,6},{8,9},{9,8},{10,11... | collective-permute-start | bytes 1572872 | tf_op jit(solution)/shard_map/ppermute | solution.py:31
  40.4 9.7 %collective-permute-start.7 = (bf16[128,2048]{1,0:T(8,128)(2,1)S(1)}, bf16[128,2048]{1,0:T(8,128)(2,1)}, u32[]{:S(2)}, u32[]{:S(2)}) collective-permute-start(bf16[128,2048]{1,0:T(8,128)(2,1)S(1)} %collective-permute-done.6.refs_2_), channel_id=1, source_target_pairs={{0,1},{1,0},{2,3},{3,2},{4,5},{5,4},{6,7},{7,6},{8,9},{9,8},{10,11... | collective-permute-start | bytes 1572872 | tf_op jit(solution)/shard_map/ppermute | solution.py:31
  52.5 9.8 %copy-start.7 = (bf16[2048,96]{0,1:T(8,128)(2,1)S(1)}, bf16[2048,96]{0,1:T(8,128)(2,1)}, u32[]{:S(2)}) copy-start(bf16[2048,96]{0,1:T(8,128)(2,1)} %param.16) | copy-start | bytes 1179652
  52.6 9.8 %copy-start.9 = (f32[2048]{0:T(1024)S(1)}, f32[2048]{0:T(1024)}, u32[]{:S(2)}) copy-start(f32[2048]{0:T(1024)} %param.15) | copy-start | bytes 24580
  52.6 57.1 %all-to-all-start.1 = ((bf16[32,8,2048]{2,1,0:T(8,128)(2,1)}), bf16[32,8,2048]{2,1,0:T(8,128)(2,1)S(1)}, u32[]{:S(2)}, u32[]{:S(2)}) async-start(bf16[32,8,2048]{2,1,0:T(8,128)(2,1)} %bitcast.128), calls=%async_computation.1 | async-start | bytes 2097152 | tf_op jit(solution)/shard_map/all_to_all | solution.py:35
  62.3 1.0 copy-start.8
  63.3 3.6 %copy-start.5 = (f32[31,96]{1,0:T(8,128)S(1)}, f32[31,96]{1,0:T(8,128)}, u32[]{:S(2)}) copy-start(f32[31,96]{1,0:T(8,128)} %param.18) | copy-start | bytes 35716
  63.3 3.6 %copy-start.2 = (s32[128,4]{0,1:T(4,128)S(1)}, s32[128,4]{0,1:T(4,128)}, u32[]{:S(2)}) copy-start(s32[128,4]{0,1:T(4,128)} %param.23) | copy-start | bytes 6148
  63.3 3.7 %copy-start.3 = (f32[128,4]{0,1:T(4,128)S(1)}, f32[128,4]{0,1:T(4,128)}, u32[]{:S(2)}) copy-start(f32[128,4]{0,1:T(4,128)} %param.24) | copy-start | bytes 6148
  63.4 43.8 %copy-start.6 = (f32[96]{0:T(128)S(1)}, f32[96]{0:T(128)}, u32[]{:S(2)}) copy-start(f32[96]{0:T(128)} %param.19) | copy-start | bytes 1156
  63.9 23.2 %collective-permute-start = (bf16[30,96]{0,1:T(8,128)(2,1)S(1)}, bf16[30,96]{0,1:T(8,128)(2,1)S(1)}, u32[]{:S(2)}, u32[]{:S(2)}) collective-permute-start(bf16[30,96]{0,1:T(8,128)(2,1)S(1)} %slice.256), channel_id=1, source_target_pairs={{0,16},{16,32},{32,48},{48,64},{64,80},{80,96},{96,112},{112,128},... | collective-permute-start | bytes 17288 | tf_op jit(solution)/shard_map/ppermute | solution.py:27
  107.6 5.1 %collective-permute-start.1 = (bf16[64,2048]{1,0:T(8,128)(2,1)S(1)}, bf16[64,2048]{1,0:T(8,128)(2,1)S(1)}, u32[]{:S(2)}, u32[]{:S(2)}) collective-permute-start(bf16[64,2048]{1,0:T(8,128)(2,1)S(1)} %fusion.15), channel_id=1, source_target_pairs={{0,1},{1,0},{2,3},{3,2},{4,5},{5,4},{6,7},{7,6},{8,9},{9,8},{10,11... | collective-permute-start | bytes 786440 | tf_op jit(solution)/shard_map/ppermute | solution.py:31
  110.4 3.4 %collective-permute-start.8 = (bf16[64,2048]{1,0:T(8,128)(2,1)S(1)}, bf16[64,2048]{1,0:T(8,128)(2,1)S(1)}, u32[]{:S(2)}, u32[]{:S(2)}) collective-permute-start(bf16[64,2048]{1,0:T(8,128)(2,1)S(1)} %fusion.16), channel_id=1, source_target_pairs={{0,1},{1,0},{2,3},{3,2},{4,5},{5,4},{6,7},{7,6},{8,9},{9,8},{10,11... | collective-permute-start | bytes 786440 | tf_op jit(solution)/shard_map/ppermute | solution.py:31
  152.4 6.6 %collective-permute-start.9 = (bf16[8,2,8,2048]{3,2,1,0:T(8,128)(2,1)S(1)}, bf16[8,2,8,2048]{3,2,1,0:T(8,128)(2,1)S(1)}, u32[]{:S(2)}, u32[]{:S(2)}) collective-permute-start(bf16[8,2,8,2048]{3,2,1,0:T(8,128)(2,1)S(1)} %all_to_all.21.own_ref), channel_id=1, source_target_pairs={{0,1},{1,0},{2,3},{3,2},{4,5},{5,4},{6,7},{7,6},{8,9},{9,8},{10,11... | collective-permute-start | bytes 1572872 | tf_op jit(solution)/shard_map/ppermute | solution.py:31
where the time goes:
time: 161 us; the launch traced here: 160 us
  blocking collectives  57.4 us (36%)
  starting transfers between devices  53.3 us (33%)
  waiting for transfers between devices  31.5 us (20%)
  Pallas kernels  10.1 us (6%)
  other arithmetic  3.93 us (2%)
  matrix products  1.88 us (1%)
    all_to_all x2, blocking collectives, exchanged(): return lax.all_to_all(x, axis, split_axis=0, concat_axis=0, tiled=True)  38.3 us
    ppermute x9, starting transfers between devices, swapped(): return lax.ppermute(x, axis, [(0, 1), (1, 0)])  28.3 us
    all_to_all x2, starting transfers between devices, exchanged(): return lax.all_to_all(x, axis, split_axis=0, concat_axis=0, tiled=True)  21.9 us
    ppermute x1, waiting for transfers between devices, shifted(): return lax.ppermute(block, axis, route)  19.8 us
    all_gather x1, blocking collectives, projected(): everyone = lax.all_gather(sums, TP)  19.1 us
    ppermute x9, waiting for transfers between devices, swapped(): return lax.ppermute(x, axis, [(0, 1), (1, 0)])  9.32 us
    pallas_call x1, Pallas kernels, hidden_units(): pl.pallas_call(hidden_kernel, in_specs=[WHOLE] * (1 + GROUP), out_specs=W...  3.46 us
  transfers between devices with their start and end apart: 12, of which 6 were waited for; matrix products, arithmetic and copies ran while one was open for 2% of the time, Pallas kernels for 4%

commit v1 on v0

--- a/solution.py
+++ b/solution.py
@@ -279,13 +279,15 @@
     slots = capacity // GROUP
     member = lax.axis_index(("y0", "c")).astype(jnp.int32)
 
-    gate_up = jnp.concatenate([expert_gate[0], expert_up[0]], axis=1)
-    down = expert_down[0]
-    gu_y = swapped(gate_up, "y0")
+    gate, up, down = expert_gate[0], expert_up[0], expert_down[0]
+    gate_y = swapped(gate, "y0")
+    up_y = swapped(up, "y0")
     down_y = swapped(down, "y0")
-    gu_c = swapped(gate_up, "c")
+    packed = jnp.concatenate([gate, up], axis=1)
+    gu_c = swapped(packed, "c")
     down_c = swapped(down, "c")
-    gu_d = swapped(gu_y, "c")
+    packed_y = jnp.concatenate([gate_y, up_y], axis=1)
+    gu_d = swapped(packed_y, "c")
     down_d = swapped(down_y, "c")
 
     ids = route_experts.T
@@ -297,7 +299,7 @@
     mixer_partial = projected(conv_out, channel_gain, w_output)
     mixer_half = core_half(mixer_partial)
 
-    hidden = hidden_units(arrived, (gate_up, gu_c, gu_y, gu_d))
+    hidden = hidden_units(arrived, (packed, gu_c, packed_y, gu_d))
     partial = projected_down(hidden, (down, down_c, down_y, down_d))
     returned = exchanged(partial.reshape(experts, slots, width), "ep").reshape(-1, width)
 

time: 161 us -> 164 us (1.019)
  starting transfers between devices: 53.3 us -> 59 us
  waiting for transfers between devices: 31.5 us -> 28.7 us
    ppermute x9 -> x10, starting transfers between devices: 28.3 us -> 34.4 us  [swapped(): return lax.ppermute(x, axis, [(0, 1), (1, 0)])]
    all_to_all x2, waiting for transfers between devices: 2.44 us -> 0.01 us  [exchanged(): return lax.all_to_all(x, axis, split_axis=0, concat_axis=0, tiled=True)]
    ppermute x9 -> x10, waiting for transfers between devices: 9.32 us -> 8.96 us  [swapped(): return lax.ppermute(x, axis, [(0, 1), (1, 0)])]
  transfers between devices with their start and end apart: 12 -> 13, of which waited for: 6 -> 5; matrix products, arithmetic and copies ran while one was open for 2% -> 3% of each run, Pallas kernels for 4% -> 4%
where the time goes in v1:
time: 164 us; the launch traced here: 163 us
  starting transfers between devices  59 us (36%)
  blocking collectives  57.3 us (35%)
  waiting for transfers between devices  28.7 us (18%)
  Pallas kernels  10.2 us (6%)
  other arithmetic  2.79 us (2%)
  local copies, waits for them, and re-layouts  2.07 us (1%)
  matrix products  1.89 us (1%)
    all_to_all x2, blocking collectives, exchanged(): return lax.all_to_all(x, axis, split_axis=0, concat_axis=0, tiled=True)  38.4 us
    ppermute x10, starting transfers between devices, swapped(): return lax.ppermute(x, axis, [(0, 1), (1, 0)])  34.4 us
    all_to_all x2, starting transfers between devices, exchanged(): return lax.all_to_all(x, axis, split_axis=0, concat_axis=0, tiled=True)  21.5 us
    ppermute x1, waiting for transfers between devices, shifted(): return lax.ppermute(block, axis, route)  19.7 us
    all_gather x1, blocking collectives, projected(): everyone = lax.all_gather(sums, TP)  18.9 us
    ppermute x10, waiting for transfers between devices, swapped(): return lax.ppermute(x, axis, [(0, 1), (1, 0)])  8.96 us
    pallas_call x1, Pallas kernels, hidden_units(): pl.pallas_call(hidden_kernel, in_specs=[WHOLE] * (1 + GROUP), out_specs=W...  3.46 us
  transfers between devices with their start and end apart: 13, of which 5 were waited for; matrix products, arithmetic and copies ran while one was open for 3% of the time, Pallas kernels for 4%

profile of v1, /device:TPU:65, one launch (start us, length us, event | category | flops | bytes accessed | tf_op | source)
XLA Modules:
  0.0 163.0 jit_solution(14141197810267458150)
XLA Ops:
  0.6 0.0 copy-start
  0.6 3.3 %collective-permute-start.3 = (bf16[2048,128]{1,0:T(8,128)(2,1)}, bf16[2048,128]{1,0:T(8,128)(2,1)S(1)}, u32[]{:S(2)}, u32[]{:S(2)}) collective-permute-start(bf16[2048,128]{1,0:T(8,128)(2,1)} %bitcast.134), channel_id=1, source_target_pairs={{0,2},{2,0},{1,3},{3,1},{4,6},{6,4},{5,7},{7,5},{8,10},{10,8},{9,1... | collective-permute-start | bytes 1572872 | tf_op jit(solution)/shard_map/ppermute | solution.py:31
  4.0 2.8 %front.1 = bf16[256,2048]{1,0:T(8,128)(2,1)} custom-call(s32[1]{0:T(128)} %bitcast.41.member, bf16[128,2048]{1,0:T(8,128)(2,1)} %x_ref.1, f32[1,2048]{1,0:T(1,128)} %bitcast.136, s32[4,128]{1,0:T(4,128)} %bitcast.125), custom_call_target="tpu_custom_call" | custom-call | tf_op jit(solution)/shard_map/front/pallas_call | solution.py:134
  6.8 12.2 %all-to-all-start = ((bf16[32,8,2048]{2,1,0:T(8,128)(2,1)}), bf16[32,8,2048]{2,1,0:T(8,128)(2,1)S(1)}, u32[]{:S(2)}, u32[]{:S(2)}) async-start(bf16[32,8,2048]{2,1,0:T(8,128)(2,1)} %bitcast.129), calls=%async_computation | async-start | bytes 2097152 | tf_op jit(solution)/shard_map/all_to_all | solution.py:35
  19.0 0.0 copy-start.1
  19.0 2.2 %collective-permute-start.4 = (bf16[2048,128]{1,0:T(8,128)(2,1)}, bf16[2048,128]{1,0:T(8,128)(2,1)S(1)}, u32[]{:S(2)}, u32[]{:S(2)}) collective-permute-start(bf16[2048,128]{1,0:T(8,128)(2,1)} %bitcast.48), channel_id=1, source_target_pairs={{0,2},{2,0},{1,3},{3,1},{4,6},{6,4},{5,7},{7,5},{8,10},{10,8},{9,1... | collective-permute-start | bytes 1572872 | tf_op jit(solution)/shard_map/ppermute | solution.py:31
  21.2 1.2 pad_maximum_fusion.refs_0_
  22.5 3.7 %collective-permute-start.2 = (bf16[2048,256]{1,0:T(8,128)(2,1)S(1)}, bf16[2048,256]{1,0:T(8,128)(2,1)S(1)}, u32[]{:S(2)}, u32[]{:S(2)}) collective-permute-start(bf16[2048,256]{1,0:T(8,128)(2,1)S(1)} %pad_maximum_fusion.refs_0_), channel_id=1, source_target_pairs={{0,1},{1,0},{2,3},{3,2},{4,5},{5,4},{6,7},{7,6},{8,9},{9,8},{10,11... | collective-permute-start | bytes 3145736 | tf_op jit(solution)/shard_map/ppermute | solution.py:31
  26.2 3.3 %collective-permute-start.7 = (bf16[128,2048]{1,0:T(8,128)(2,1)S(1)}, bf16[128,2048]{1,0:T(8,128)(2,1)S(1)}, u32[]{:S(2)}, u32[]{:S(2)}) collective-permute-start(bf16[128,2048]{1,0:T(8,128)(2,1)S(1)} %bitcast.122), channel_id=1, source_target_pairs={{0,2},{2,0},{1,3},{3,1},{4,6},{6,4},{5,7},{7,5},{8,10},{10,8},{9,1... | collective-permute-start | bytes 1572872 | tf_op jit(solution)/shard_map/ppermute | solution.py:31
  29.5 0.1 constant_dynamic-update-slice_fusion.1
  29.6 3.6 %collective-permute-done.4 = bf16[2048,128]{1,0:T(8,128)(2,1)S(1)} collective-permute-done((bf16[2048,128]{1,0:T(8,128)(2,1)}, bf16[2048,128]{1,0:T(8,128)(2,1)S(1)}, u32[]{:S(2)}, u32[]{:S(2)}) %collective-permute-start.4) | collective-permute-done | bytes 524320 | tf_op jit(solution)/shard_map/ppermute | solution.py:31
  33.2 0.1 constant_dynamic-update-slice_fusion.refs_2_
  33.4 6.2 %collective-permute-start.5 = (bf16[2048,256]{1,0:T(8,128)(2,1)S(1)}, bf16[2048,256]{1,0:T(8,128)(2,1)}, u32[]{:S(2)}, u32[]{:S(2)}) collective-permute-start(bf16[2048,256]{1,0:T(8,128)(2,1)S(1)} %constant_dynamic-update-slice_fusion.refs_2_), channel_id=1, source_target_pairs={{0,1},{1,0},{2,3},{3,2},{4,5},{5,4},{6,7},{7,6},{8,9},{9,8},{10,11... | collective-permute-start | bytes 3145736 | tf_op jit(solution)/shard_map/ppermute | solution.py:31
  39.6 1.9 %collective-permute-start.6 = (bf16[128,2048]{1,0:T(8,128)(2,1)S(1)}, bf16[128,2048]{1,0:T(8,128)(2,1)S(1)}, u32[]{:S(2)}, u32[]{:S(2)}) collective-permute-start(bf16[128,2048]{1,0:T(8,128)(2,1)S(1)} %bitcast.123), channel_id=1, source_target_pairs={{0,1},{1,0},{2,3},{3,2},{4,5},{5,4},{6,7},{7,6},{8,9},{9,8},{10,11... | collective-permute-start | bytes 1572872 | tf_op jit(solution)/shard_map/ppermute | solution.py:31
  41.6 0.2 convert_reduce_fusion
  41.7 2.7 %collective-permute-done.7.refs_2_ = bf16[128,2048]{1,0:T(8,128)(2,1)S(1)} collective-permute-done((bf16[128,2048]{1,0:T(8,128)(2,1)S(1)}, bf16[128,2048]{1,0:T(8,128)(2,1)S(1)}, u32[]{:S(2)}, u32[]{:S(2)}) %collective-permute-start.7) | collective-permute-done | bytes 524320 | tf_op jit(solution)/shard_map/ppermute | solution.py:31
  44.5 4.3 %collective-permute-start.8 = (bf16[128,2048]{1,0:T(8,128)(2,1)S(1)}, bf16[128,2048]{1,0:T(8,128)(2,1)}, u32[]{:S(2)}, u32[]{:S(2)}) collective-permute-start(bf16[128,2048]{1,0:T(8,128)(2,1)S(1)} %collective-permute-done.7.refs_2_), channel_id=1, source_target_pairs={{0,1},{1,0},{2,3},{3,2},{4,5},{5,4},{6,7},{7,6},{8,9},{9,8},{10,11... | collective-permute-start | bytes 1572872 | tf_op jit(solution)/shard_map/ppermute | solution.py:31
  48.7 0.3 fusion.7
  49.1 1.0 copy-done.7
  50.1 3.5 %hidden.1.hidden_ref = bf16[256,512]{1,0:T(8,128)(2,1)S(1)} custom-call(bf16[256,2048]{1,0:T(8,128)(2,1)S(1)} %bitcast.121, bf16[2048,256]{1,0:T(8,128)(2,1)} %copy-done.4, bf16[2048,256]{1,0:T(8,128)(2,1)} %copy-done.7, bf16[2048,256]{1,0:T(8,128)(2,1)} %copy-done.5, bf16[2048,256]{1,0:T(8,128)(2,1)} %collective-permute-done.5.refs_3_), custom_call_target="tpu_custom_call" | custom-call | tf_op jit(solution)/shard_map/hidden/pallas_call | solution.py:210
  53.5 2.5 %project.1 = bf16[256,2048]{1,0:T(8,128)(2,1)} custom-call(bf16[256,512]{1,0:T(8,128)(2,1)S(1)} %hidden.1.hidden_ref, bf16[128,2048]{1,0:T(8,128)(2,1)S(1)} %bitcast.124, bf16[128,2048]{1,0:T(8,128)(2,1)S(1)} %collective-permute-done.6.refs_1_, bf16[128,2048]{1,0:T(8,128)(2,1)S(1)} %collective-permute-done.7.refs_2_, ...), custom_call_target="tpu_custom_call" | custom-call | tf_op jit(solution)/shard_map/project/pallas_call | solution.py:222
  56.1 0.0 copy-start.11
  56.1 9.4 %all-to-all-start.1 = ((bf16[32,8,2048]{2,1,0:T(8,128)(2,1)}), bf16[32,8,2048]{2,1,0:T(8,128)(2,1)S(1)}, u32[]{:S(2)}, u32[]{:S(2)}) async-start(bf16[32,8,2048]{2,1,0:T(8,128)(2,1)} %bitcast.128), calls=%async_computation.1 | async-start | bytes 2097152 | tf_op jit(solution)/shard_map/all_to_all | solution.py:35
  65.5 0.0 copy-start.12
  65.5 0.4 fusion.57
  65.9 0.6 copy-done.12
  66.5 0.4 fusion.6
  66.9 0.1 slice.256
  67.0 3.1 %collective-permute-start = (bf16[30,96]{0,1:T(8,128)(2,1)S(1)}, bf16[30,96]{0,1:T(8,128)(2,1)S(1)}, u32[]{:S(2)}, u32[]{:S(2)}) collective-permute-start(bf16[30,96]{0,1:T(8,128)(2,1)S(1)} %slice.256), channel_id=1, source_target_pairs={{0,16},{16,32},{32,48},{48,64},{64,80},{80,96},{96,112},{112,128},... | collective-permute-start | bytes 17288 | tf_op jit(solution)/shard_map/ppermute | solution.py:27
  70.2 0.3 mixing.1
  70.5 19.7 %collective-permute-done = bf16[30,96]{0,1:T(8,128)(2,1)S(1)} collective-permute-done((bf16[30,96]{0,1:T(8,128)(2,1)S(1)}, bf16[30,96]{0,1:T(8,128)(2,1)S(1)}, u32[]{:S(2)}, u32[]{:S(2)}) %collective-permute-start) | collective-permute-done | bytes 5792 | tf_op jit(solution)/shard_map/ppermute | solution.py:27
  90.2 0.9 fusion.59
  91.1 18.9 %all-gather.1 = f32[16,2,128]{2,1,0:T(2,128)S(1)} all-gather(f32[1,2,128]{2,1,0:T(2,128)S(1)} %maximum_bitcast_fusion), channel_id=2, replica_groups=mesh['ep'=32,'y2'=2,'y1'=2,'y0'=2,'c'=2] {'y2','y1','y0','c'}, dimensions={0}, use_global_device_ids=true | all-gather | bytes 17408 | tf_op jit(solution)/shard_map/all_gather | solution.py:85
  110.1 0.4 fusion.19
  110.5 2.1 %collective-permute-start.1 = (bf16[64,2048]{1,0:T(8,128)(2,1)S(1)}, bf16[64,2048]{1,0:T(8,128)(2,1)S(1)}, u32[]{:S(2)}, u32[]{:S(2)}) collective-permute-start(bf16[64,2048]{1,0:T(8,128)(2,1)S(1)} %fusion.15), channel_id=1, source_target_pairs={{0,1},{1,0},{2,3},{3,2},{4,5},{5,4},{6,7},{7,6},{8,9},{9,8},{10,11... | collective-permute-start | bytes 786440 | tf_op jit(solution)/shard_map/ppermute | solution.py:31
  112.6 0.3 fusion.10
  113.0 0.3 convolution_add_fusion
  113.3 2.2 %collective-permute-start.9 = (bf16[64,2048]{1,0:T(8,128)(2,1)S(1)}, bf16[64,2048]{1,0:T(8,128)(2,1)S(1)}, u32[]{:S(2)}, u32[]{:S(2)}) collective-permute-start(bf16[64,2048]{1,0:T(8,128)(2,1)S(1)} %fusion.16), channel_id=1, source_target_pairs={{0,1},{1,0},{2,3},{3,2},{4,5},{5,4},{6,7},{7,6},{8,9},{9,8},{10,11... | collective-permute-start | bytes 786440 | tf_op jit(solution)/shard_map/ppermute | solution.py:31
  115.6 0.1 fusion.17
  115.7 1.1 collective-permute-done.9
  116.8 0.1 fusion.18
  116.8 0.1 pad_maximum_fusion.1
  116.9 20.7 %all_to_all.20 = bf16[8,2,8,2048]{3,2,1,0:T(8,128)(2,1)S(1)} all-to-all(bf16[8,2,8,2048]{3,2,1,0:T(8,128)(2,1)S(1)} %pad_maximum_fusion.1), channel_id=1, replica_groups=mesh['ep'=32,'y2'=2,'y1'=2,'y0'=2,'c'=2] {'y2','y1','y0'}, dimensions={0} | all-to-all | bytes 1048576 | tf_op jit(solution)/shard_map/all_to_all | solution.py:35
  137.6 0.1 reduce_sum.62
  137.7 17.7 %all_to_all.21.own_ref = bf16[8,2,8,2048]{3,2,1,0:T(8,128)(2,1)S(1)} all-to-all(bf16[8,2,8,2048]{3,2,1,0:T(8,128)(2,1)S(1)} %broadcast_in_dim.2), channel_id=1, replica_groups=mesh['ep'=32,'y2'=2,'y1'=2,'y0'=2,'c'=2] {'y2','y1','y0'}, dimensions={0} | all-to-all | bytes 1048576 | tf_op jit(solution)/shard_map/all_to_all | solution.py:35
  155.5 5.0 %collective-permute-start.10 = (bf16[8,2,8,2048]{3,2,1,0:T(8,128)(2,1)S(1)}, bf16[8,2,8,2048]{3,2,1,0:T(8,128)(2,1)S(1)}, u32[]{:S(2)}, u32[]{:S(2)}) collective-permute-start(bf16[8,2,8,2048]{3,2,1,0:T(8,128)(2,1)S(1)} %all_to_all.21.own_ref), channel_id=1, source_target_pairs={{0,1},{1,0},{2,3},{3,2},{4,5},{5,4},{6,7},{7,6},{8,9},{9,8},{10,11... | collective-permute-start | bytes 1572872 | tf_op jit(solution)/shard_map/ppermute | solution.py:31
  160.5 1.5 collective-permute-done.10.other_ref
  162.0 1.0 placing.1
  (41 shorter events, 0.3 us)
Async XLA Ops:
  0.6 109.4 %copy-start = (bf16[96,2048]{1,0:T(8,128)(2,1)S(1)}, bf16[96,2048]{1,0:T(8,128)(2,1)}, u32[]{:S(2)}) copy-start(bf16[96,2048]{1,0:T(8,128)(2,1)} %param.20) | copy-start | bytes 1179652
  0.6 28.9 %collective-permute-start.3 = (bf16[2048,128]{1,0:T(8,128)(2,1)}, bf16[2048,128]{1,0:T(8,128)(2,1)S(1)}, u32[]{:S(2)}, u32[]{:S(2)}) collective-permute-start(bf16[2048,128]{1,0:T(8,128)(2,1)} %bitcast.134), channel_id=1, source_target_pairs={{0,2},{2,0},{1,3},{3,1},{4,6},{6,4},{5,7},{7,5},{8,10},{10,8},{9,1... | collective-permute-start | bytes 1572872 | tf_op jit(solution)/shard_map/ppermute | solution.py:31
  6.8 14.4 %copy-start.8 = (bf16[1,2048,128]{2,1,0:T(8,128)(2,1)S(1)}, bf16[1,2048,128]{2,1,0:T(8,128)(2,1)}, u32[]{:S(2)}) copy-start(bf16[1,2048,128]{2,1,0:T(8,128)(2,1)} %param.25) | copy-start | bytes 1572868
  6.8 43.2 %all-to-all-start = ((bf16[32,8,2048]{2,1,0:T(8,128)(2,1)}), bf16[32,8,2048]{2,1,0:T(8,128)(2,1)S(1)}, u32[]{:S(2)}, u32[]{:S(2)}) async-start(bf16[32,8,2048]{2,1,0:T(8,128)(2,1)} %bitcast.129), calls=%async_computation | async-start | bytes 2097152 | tf_op jit(solution)/shard_map/all_to_all | solution.py:35
  19.0 7.2 %copy-start.1 = (bf16[1,128,2048]{2,1,0:T(8,128)(2,1)S(1)}, bf16[1,128,2048]{2,1,0:T(8,128)(2,1)}, u32[]{:S(2)}) copy-start(bf16[1,128,2048]{2,1,0:T(8,128)(2,1)} %param.27) | copy-start | bytes 1572868
  19.0 14.2 %collective-permute-start.4 = (bf16[2048,128]{1,0:T(8,128)(2,1)}, bf16[2048,128]{1,0:T(8,128)(2,1)S(1)}, u32[]{:S(2)}, u32[]{:S(2)}) collective-permute-start(bf16[2048,128]{1,0:T(8,128)(2,1)} %bitcast.48), channel_id=1, source_target_pairs={{0,2},{2,0},{1,3},{3,1},{4,6},{6,4},{5,7},{7,5},{8,10},{10,8},{9,1... | collective-permute-start | bytes 1572872 | tf_op jit(solution)/shard_map/ppermute | solution.py:31
  22.4 10.9 %copy-start.4 = (bf16[2048,256]{1,0:T(8,128)(2,1)}, bf16[2048,256]{1,0:T(8,128)(2,1)S(1)}, u32[]{:S(2)}) copy-start(bf16[2048,256]{1,0:T(8,128)(2,1)S(1)} %pad_maximum_fusion.refs_0_) | copy-start | bytes 3145732
  22.5 26.6 %collective-permute-start.2 = (bf16[2048,256]{1,0:T(8,128)(2,1)S(1)}, bf16[2048,256]{1,0:T(8,128)(2,1)S(1)}, u32[]{:S(2)}, u32[]{:S(2)}) collective-permute-start(bf16[2048,256]{1,0:T(8,128)(2,1)S(1)} %pad_maximum_fusion.refs_0_), channel_id=1, source_target_pairs={{0,1},{1,0},{2,3},{3,2},{4,5},{5,4},{6,7},{7,6},{8,9},{9,8},{10,11... | collective-permute-start | bytes 3145736 | tf_op jit(solution)/shard_map/ppermute | solution.py:31
  26.2 15.4 %copy-start.6 = (bf16[128,2048]{1,0:T(8,128)(2,1)S(1)}, bf16[128,2048]{1,0:T(8,128)(2,1)}, u32[]{:S(2)}) copy-start(bf16[128,2048]{1,0:T(8,128)(2,1)} %param.14) | copy-start | bytes 1572868
  26.2 18.3 %collective-permute-start.7 = (bf16[128,2048]{1,0:T(8,128)(2,1)S(1)}, bf16[128,2048]{1,0:T(8,128)(2,1)S(1)}, u32[]{:S(2)}, u32[]{:S(2)}) collective-permute-start(bf16[128,2048]{1,0:T(8,128)(2,1)S(1)} %bitcast.122), channel_id=1, source_target_pairs={{0,2},{2,0},{1,3},{3,1},{4,6},{6,4},{5,7},{7,5},{8,10},{10,8},{9,1... | collective-permute-start | bytes 1572872 | tf_op jit(solution)/shard_map/ppermute | solution.py:31
  33.4 15.7 %copy-start.5 = (bf16[2048,256]{1,0:T(8,128)(2,1)}, bf16[2048,256]{1,0:T(8,128)(2,1)S(1)}, u32[]{:S(2)}) copy-start(bf16[2048,256]{1,0:T(8,128)(2,1)S(1)} %constant_dynamic-update-slice_fusion.refs_2_) | copy-start | bytes 3145732
  33.4 16.7 %collective-permute-start.5 = (bf16[2048,256]{1,0:T(8,128)(2,1)S(1)}, bf16[2048,256]{1,0:T(8,128)(2,1)}, u32[]{:S(2)}, u32[]{:S(2)}) collective-permute-start(bf16[2048,256]{1,0:T(8,128)(2,1)S(1)} %constant_dynamic-update-slice_fusion.refs_2_), channel_id=1, source_target_pairs={{0,1},{1,0},{2,3},{3,2},{4,5},{5,4},{6,7},{7,6},{8,9},{9,8},{10,11... | collective-permute-start | bytes 3145736 | tf_op jit(solution)/shard_map/ppermute | solution.py:31
  39.6 13.9 %collective-permute-start.6 = (bf16[128,2048]{1,0:T(8,128)(2,1)S(1)}, bf16[128,2048]{1,0:T(8,128)(2,1)S(1)}, u32[]{:S(2)}, u32[]{:S(2)}) collective-permute-start(bf16[128,2048]{1,0:T(8,128)(2,1)S(1)} %bitcast.123), channel_id=1, source_target_pairs={{0,1},{1,0},{2,3},{3,2},{4,5},{5,4},{6,7},{7,6},{8,9},{9,8},{10,11... | collective-permute-start | bytes 1572872 | tf_op jit(solution)/shard_map/ppermute | solution.py:31
  44.5 9.1 %collective-permute-start.8 = (bf16[128,2048]{1,0:T(8,128)(2,1)S(1)}, bf16[128,2048]{1,0:T(8,128)(2,1)}, u32[]{:S(2)}, u32[]{:S(2)}) collective-permute-start(bf16[128,2048]{1,0:T(8,128)(2,1)S(1)} %collective-permute-done.7.refs_2_), channel_id=1, source_target_pairs={{0,1},{1,0},{2,3},{3,2},{4,5},{5,4},{6,7},{7,6},{8,9},{9,8},{10,11... | collective-permute-start | bytes 1572872 | tf_op jit(solution)/shard_map/ppermute | solution.py:31
  49.1 1.0 copy-start.7
  56.1 9.4 %copy-start.11 = (bf16[2048,96]{0,1:T(8,128)(2,1)S(1)}, bf16[2048,96]{0,1:T(8,128)(2,1)}, u32[]{:S(2)}) copy-start(bf16[2048,96]{0,1:T(8,128)(2,1)} %param.16) | copy-start | bytes 1179652
  56.1 9.4 %copy-start.13 = (f32[2048]{0:T(1024)S(1)}, f32[2048]{0:T(1024)}, u32[]{:S(2)}) copy-start(f32[2048]{0:T(1024)} %param.15) | copy-start | bytes 24580
  56.1 56.5 %all-to-all-start.1 = ((bf16[32,8,2048]{2,1,0:T(8,128)(2,1)}), bf16[32,8,2048]{2,1,0:T(8,128)(2,1)S(1)}, u32[]{:S(2)}, u32[]{:S(2)}) async-start(bf16[32,8,2048]{2,1,0:T(8,128)(2,1)} %bitcast.128), calls=%async_computation.1 | async-start | bytes 2097152 | tf_op jit(solution)/shard_map/all_to_all | solution.py:35
  65.5 1.0 copy-start.12
  66.5 3.6 %copy-start.9 = (f32[31,96]{1,0:T(8,128)S(1)}, f32[31,96]{1,0:T(8,128)}, u32[]{:S(2)}) copy-start(f32[31,96]{1,0:T(8,128)} %param.18) | copy-start | bytes 35716
  66.5 3.6 %copy-start.2 = (s32[128,4]{0,1:T(4,128)S(1)}, s32[128,4]{0,1:T(4,128)}, u32[]{:S(2)}) copy-start(s32[128,4]{0,1:T(4,128)} %param.23) | copy-start | bytes 6148
  66.5 3.7 %copy-start.3 = (f32[128,4]{0,1:T(4,128)S(1)}, f32[128,4]{0,1:T(4,128)}, u32[]{:S(2)}) copy-start(f32[128,4]{0,1:T(4,128)} %param.24) | copy-start | bytes 6148
  66.5 43.6 %copy-start.10 = (f32[96]{0:T(128)S(1)}, f32[96]{0:T(128)}, u32[]{:S(2)}) copy-start(f32[96]{0:T(128)} %param.19) | copy-start | bytes 1156
  67.0 23.2 %collective-permute-start = (bf16[30,96]{0,1:T(8,128)(2,1)S(1)}, bf16[30,96]{0,1:T(8,128)(2,1)S(1)}, u32[]{:S(2)}, u32[]{:S(2)}) collective-permute-start(bf16[30,96]{0,1:T(8,128)(2,1)S(1)} %slice.256), channel_id=1, source_target_pairs={{0,16},{16,32},{32,48},{48,64},{64,80},{80,96},{96,112},{112,128},... | collective-permute-start | bytes 17288 | tf_op jit(solution)/shard_map/ppermute | solution.py:27
  110.5 5.1 %collective-permute-start.1 = (bf16[64,2048]{1,0:T(8,128)(2,1)S(1)}, bf16[64,2048]{1,0:T(8,128)(2,1)S(1)}, u32[]{:S(2)}, u32[]{:S(2)}) collective-permute-start(bf16[64,2048]{1,0:T(8,128)(2,1)S(1)} %fusion.15), channel_id=1, source_target_pairs={{0,1},{1,0},{2,3},{3,2},{4,5},{5,4},{6,7},{7,6},{8,9},{9,8},{10,11... | collective-permute-start | bytes 786440 | tf_op jit(solution)/shard_map/ppermute | solution.py:31
  113.3 3.4 %collective-permute-start.9 = (bf16[64,2048]{1,0:T(8,128)(2,1)S(1)}, bf16[64,2048]{1,0:T(8,128)(2,1)S(1)}, u32[]{:S(2)}, u32[]{:S(2)}) collective-permute-start(bf16[64,2048]{1,0:T(8,128)(2,1)S(1)} %fusion.16), channel_id=1, source_target_pairs={{0,1},{1,0},{2,3},{3,2},{4,5},{5,4},{6,7},{7,6},{8,9},{9,8},{10,11... | collective-permute-start | bytes 786440 | tf_op jit(solution)/shard_map/ppermute | solution.py:31
  155.5 6.6 %collective-permute-start.10 = (bf16[8,2,8,2048]{3,2,1,0:T(8,128)(2,1)S(1)}, bf16[8,2,8,2048]{3,2,1,0:T(8,128)(2,1)S(1)}, u32[]{:S(2)}, u32[]{:S(2)}) collective-permute-start(bf16[8,2,8,2048]{3,2,1,0:T(8,128)(2,1)S(1)} %all_to_all.21.own_ref), channel_id=1, source_target_pairs={{0,1},{1,0},{2,3},{3,2},{4,5},{5,4},{6,7},{7,6},{8,9},{9,8},{10,11... | collective-permute-start | bytes 1572872 | tf_op jit(solution)/shard_map/ppermute | solution.py:31

commit v2 on v1

--- a/solution.py
+++ b/solution.py
@@ -117,15 +117,26 @@
     return jnp.dot(spread, place, preferred_element_type=jnp.float32) == slot.astype(jnp.float32)
 
 
-def front_kernel(member, x_ref, gain_ref, ids_ref, rows_ref):
+def front_kernel(member, x_ref, gain_ref, ids_ref, out_hbm, out_buf, sems):
     rows = x_ref.shape[0]
-    sent = rows_ref.shape[0]
+    sent, width = out_hbm.shape
     slots = sent // EXPERTS
     normed = row_norm(x_ref[...], gain_ref[...]).astype(jnp.bfloat16)
     _, place = places(ids_ref, rows)
     taken = taken_by(place, spread_over(sent, slots), slots, member[0])
     select = jnp.where(taken, 1.0, 0.0).astype(jnp.bfloat16)
-    rows_ref[...] = jnp.dot(select, normed, preferred_element_type=jnp.float32).astype(jnp.bfloat16)
+    parts = sems.shape[0]
+    step = width // parts
+    copies = []
+    for part in range(parts):
+        own = slice(part * step, (part + 1) * step)
+        out_buf[:, own] = jnp.dot(
+            select, normed[:, own], preferred_element_type=jnp.float32
+        ).astype(jnp.bfloat16)
+        copies.append(pltpu.make_async_copy(out_buf.at[:, own], out_hbm.at[:, own], sems.at[part]))
+        copies[-1].start()
+    for copy in copies:
+        copy.wait()
 
 
 def front(member, x, gain, ids, sent):
@@ -134,8 +145,9 @@
     return pl.pallas_call(
         front_kernel,
         in_specs=[pl.BlockSpec(memory_space=pltpu.SMEM)] + [whole] * 3,
-        out_specs=whole,
+        out_specs=pl.BlockSpec(memory_space=pl.ANY),
         out_shape=jax.ShapeDtypeStruct((sent, width), jnp.bfloat16),
+        scratch_shapes=[pltpu.VMEM((sent, width), jnp.bfloat16), pltpu.SemaphoreType.DMA((4,))],
         compiler_params=pltpu.CompilerParams(vmem_limit_bytes=57000 << 10),
         name="front",
     )(member.reshape(1), x, gain.reshape(1, width), ids)

time: 164 us -> 164 us (level)
  no operation moved by 1% of the time
where the time goes in v2:
time: 164 us; the launch traced here: 163 us
  starting transfers between devices  59 us (36%)
  blocking collectives  57.3 us (35%)
  waiting for transfers between devices  28.7 us (18%)
  Pallas kernels  10 us (6%)
  other arithmetic  2.79 us (2%)
  local copies, waits for them, and re-layouts  2.07 us (1%)
  matrix products  1.89 us (1%)
    all_to_all x2, blocking collectives, exchanged(): return lax.all_to_all(x, axis, split_axis=0, concat_axis=0, tiled=True)  38.4 us
    ppermute x10, starting transfers between devices, swapped(): return lax.ppermute(x, axis, [(0, 1), (1, 0)])  34.4 us
    all_to_all x2, starting transfers between devices, exchanged(): return lax.all_to_all(x, axis, split_axis=0, concat_axis=0, tiled=True)  21.5 us
    ppermute x1, waiting for transfers between devices, shifted(): return lax.ppermute(block, axis, route)  19.7 us
    all_gather x1, blocking collectives, projected(): everyone = lax.all_gather(sums, TP)  18.9 us
    ppermute x10, waiting for transfers between devices, swapped(): return lax.ppermute(x, axis, [(0, 1), (1, 0)])  8.94 us
    pallas_call x1, Pallas kernels, hidden_units(): pl.pallas_call(hidden_kernel, in_specs=[WHOLE] * (1 + GROUP), out_specs=W...  3.46 us
  transfers between devices with their start and end apart: 13, of which 5 were waited for; matrix products, arithmetic and copies ran while one was open for 3% of the time, Pallas kernels for 4%

profile of v2, /device:TPU:65, one launch (start us, length us, event | category | flops | bytes accessed | tf_op | source)
XLA Modules:
  0.0 162.9 jit_solution(7121874885839511861)
XLA Ops:
  0.6 0.0 copy-start
  0.6 3.3 %collective-permute-start.3 = (bf16[2048,128]{1,0:T(8,128)(2,1)}, bf16[2048,128]{1,0:T(8,128)(2,1)S(1)}, u32[]{:S(2)}, u32[]{:S(2)}) collective-permute-start(bf16[2048,128]{1,0:T(8,128)(2,1)} %bitcast.134), channel_id=1, source_target_pairs={{0,2},{2,0},{1,3},{3,1},{4,6},{6,4},{5,7},{7,5},{8,10},{10,8},{9,1... | collective-permute-start | bytes 1572872 | tf_op jit(solution)/shard_map/ppermute | solution.py:31
  4.0 2.7 %front.1 = bf16[256,2048]{1,0:T(8,128)(2,1)} custom-call(s32[1]{0:T(128)} %bitcast.41.member, bf16[128,2048]{1,0:T(8,128)(2,1)} %x_ref.1, f32[1,2048]{1,0:T(1,128)} %bitcast.136, s32[4,128]{1,0:T(4,128)} %bitcast.125), custom_call_target="tpu_custom_call" | custom-call | tf_op jit(solution)/shard_map/front/pallas_call | solution.py:145
  6.7 0.0 copy-start.8
  6.7 12.2 %all-to-all-start = ((bf16[32,8,2048]{2,1,0:T(8,128)(2,1)}), bf16[32,8,2048]{2,1,0:T(8,128)(2,1)S(1)}, u32[]{:S(2)}, u32[]{:S(2)}) async-start(bf16[32,8,2048]{2,1,0:T(8,128)(2,1)} %bitcast.129), calls=%async_computation | async-start | bytes 2097152 | tf_op jit(solution)/shard_map/all_to_all | solution.py:35
  18.9 0.0 copy-start.1
  18.9 2.2 %collective-permute-start.4 = (bf16[2048,128]{1,0:T(8,128)(2,1)}, bf16[2048,128]{1,0:T(8,128)(2,1)S(1)}, u32[]{:S(2)}, u32[]{:S(2)}) collective-permute-start(bf16[2048,128]{1,0:T(8,128)(2,1)} %bitcast.48), channel_id=1, source_target_pairs={{0,2},{2,0},{1,3},{3,1},{4,6},{6,4},{5,7},{7,5},{8,10},{10,8},{9,1... | collective-permute-start | bytes 1572872 | tf_op jit(solution)/shard_map/ppermute | solution.py:31
  21.1 1.2 pad_maximum_fusion.refs_0_
  22.3 3.7 %collective-permute-start.2 = (bf16[2048,256]{1,0:T(8,128)(2,1)S(1)}, bf16[2048,256]{1,0:T(8,128)(2,1)S(1)}, u32[]{:S(2)}, u32[]{:S(2)}) collective-permute-start(bf16[2048,256]{1,0:T(8,128)(2,1)S(1)} %pad_maximum_fusion.refs_0_), channel_id=1, source_target_pairs={{0,1},{1,0},{2,3},{3,2},{4,5},{5,4},{6,7},{7,6},{8,9},{9,8},{10,11... | collective-permute-start | bytes 3145736 | tf_op jit(solution)/shard_map/ppermute | solution.py:31
  26.1 3.3 %collective-permute-start.7 = (bf16[128,2048]{1,0:T(8,128)(2,1)S(1)}, bf16[128,2048]{1,0:T(8,128)(2,1)S(1)}, u32[]{:S(2)}, u32[]{:S(2)}) collective-permute-start(bf16[128,2048]{1,0:T(8,128)(2,1)S(1)} %bitcast.122), channel_id=1, source_target_pairs={{0,2},{2,0},{1,3},{3,1},{4,6},{6,4},{5,7},{7,5},{8,10},{10,8},{9,1... | collective-permute-start | bytes 1572872 | tf_op jit(solution)/shard_map/ppermute | solution.py:31
  29.4 0.1 constant_dynamic-update-slice_fusion.1
  29.5 3.6 %collective-permute-done.4 = bf16[2048,128]{1,0:T(8,128)(2,1)S(1)} collective-permute-done((bf16[2048,128]{1,0:T(8,128)(2,1)}, bf16[2048,128]{1,0:T(8,128)(2,1)S(1)}, u32[]{:S(2)}, u32[]{:S(2)}) %collective-permute-start.4) | collective-permute-done | bytes 524320 | tf_op jit(solution)/shard_map/ppermute | solution.py:31
  33.1 0.1 constant_dynamic-update-slice_fusion.refs_2_
  33.2 6.2 %collective-permute-start.5 = (bf16[2048,256]{1,0:T(8,128)(2,1)S(1)}, bf16[2048,256]{1,0:T(8,128)(2,1)}, u32[]{:S(2)}, u32[]{:S(2)}) collective-permute-start(bf16[2048,256]{1,0:T(8,128)(2,1)S(1)} %constant_dynamic-update-slice_fusion.refs_2_), channel_id=1, source_target_pairs={{0,1},{1,0},{2,3},{3,2},{4,5},{5,4},{6,7},{7,6},{8,9},{9,8},{10,11... | collective-permute-start | bytes 3145736 | tf_op jit(solution)/shard_map/ppermute | solution.py:31
  39.5 1.9 %collective-permute-start.6 = (bf16[128,2048]{1,0:T(8,128)(2,1)S(1)}, bf16[128,2048]{1,0:T(8,128)(2,1)S(1)}, u32[]{:S(2)}, u32[]{:S(2)}) collective-permute-start(bf16[128,2048]{1,0:T(8,128)(2,1)S(1)} %bitcast.123), channel_id=1, source_target_pairs={{0,1},{1,0},{2,3},{3,2},{4,5},{5,4},{6,7},{7,6},{8,9},{9,8},{10,11... | collective-permute-start | bytes 1572872 | tf_op jit(solution)/shard_map/ppermute | solution.py:31
  41.4 0.2 convert_reduce_fusion
  41.6 2.7 %collective-permute-done.7.refs_2_ = bf16[128,2048]{1,0:T(8,128)(2,1)S(1)} collective-permute-done((bf16[128,2048]{1,0:T(8,128)(2,1)S(1)}, bf16[128,2048]{1,0:T(8,128)(2,1)S(1)}, u32[]{:S(2)}, u32[]{:S(2)}) %collective-permute-start.7) | collective-permute-done | bytes 524320 | tf_op jit(solution)/shard_map/ppermute | solution.py:31
  44.3 4.3 %collective-permute-start.8 = (bf16[128,2048]{1,0:T(8,128)(2,1)S(1)}, bf16[128,2048]{1,0:T(8,128)(2,1)}, u32[]{:S(2)}, u32[]{:S(2)}) collective-permute-start(bf16[128,2048]{1,0:T(8,128)(2,1)S(1)} %collective-permute-done.7.refs_2_), channel_id=1, source_target_pairs={{0,1},{1,0},{2,3},{3,2},{4,5},{5,4},{6,7},{7,6},{8,9},{9,8},{10,11... | collective-permute-start | bytes 1572872 | tf_op jit(solution)/shard_map/ppermute | solution.py:31
  48.6 0.3 fusion.7
  48.9 1.0 copy-done.7
  49.9 3.5 %hidden.1.hidden_ref = bf16[256,512]{1,0:T(8,128)(2,1)S(1)} custom-call(bf16[256,2048]{1,0:T(8,128)(2,1)S(1)} %bitcast.121, bf16[2048,256]{1,0:T(8,128)(2,1)} %copy-done.4, bf16[2048,256]{1,0:T(8,128)(2,1)} %copy-done.7, bf16[2048,256]{1,0:T(8,128)(2,1)} %copy-done.5, bf16[2048,256]{1,0:T(8,128)(2,1)} %collective-permute-done.5.refs_3_), custom_call_target="tpu_custom_call" | custom-call | tf_op jit(solution)/shard_map/hidden/pallas_call | solution.py:222
  53.4 2.5 %project.1 = bf16[256,2048]{1,0:T(8,128)(2,1)} custom-call(bf16[256,512]{1,0:T(8,128)(2,1)S(1)} %hidden.1.hidden_ref, bf16[128,2048]{1,0:T(8,128)(2,1)S(1)} %bitcast.124, bf16[128,2048]{1,0:T(8,128)(2,1)S(1)} %collective-permute-done.6.refs_1_, bf16[128,2048]{1,0:T(8,128)(2,1)S(1)} %collective-permute-done.7.refs_2_, ...), custom_call_target="tpu_custom_call" | custom-call | tf_op jit(solution)/shard_map/project/pallas_call | solution.py:234
  56.0 9.4 %all-to-all-start.1 = ((bf16[32,8,2048]{2,1,0:T(8,128)(2,1)}), bf16[32,8,2048]{2,1,0:T(8,128)(2,1)S(1)}, u32[]{:S(2)}, u32[]{:S(2)}) async-start(bf16[32,8,2048]{2,1,0:T(8,128)(2,1)} %bitcast.128), calls=%async_computation.1 | async-start | bytes 2097152 | tf_op jit(solution)/shard_map/all_to_all | solution.py:35
  65.4 0.0 copy-start.12
  65.4 0.4 fusion.57
  65.8 0.6 copy-done.12
  66.4 0.4 fusion.6
  66.8 0.1 slice.256
  66.9 3.1 %collective-permute-start = (bf16[30,96]{0,1:T(8,128)(2,1)S(1)}, bf16[30,96]{0,1:T(8,128)(2,1)S(1)}, u32[]{:S(2)}, u32[]{:S(2)}) collective-permute-start(bf16[30,96]{0,1:T(8,128)(2,1)S(1)} %slice.256), channel_id=1, source_target_pairs={{0,16},{16,32},{32,48},{48,64},{64,80},{80,96},{96,112},{112,128},... | collective-permute-start | bytes 17288 | tf_op jit(solution)/shard_map/ppermute | solution.py:27
  70.0 0.3 mixing.1
  70.4 19.7 %collective-permute-done = bf16[30,96]{0,1:T(8,128)(2,1)S(1)} collective-permute-done((bf16[30,96]{0,1:T(8,128)(2,1)S(1)}, bf16[30,96]{0,1:T(8,128)(2,1)S(1)}, u32[]{:S(2)}, u32[]{:S(2)}) %collective-permute-start) | collective-permute-done | bytes 5792 | tf_op jit(solution)/shard_map/ppermute | solution.py:27
  90.1 0.9 fusion.59
  91.0 18.9 %all-gather.1 = f32[16,2,128]{2,1,0:T(2,128)S(1)} all-gather(f32[1,2,128]{2,1,0:T(2,128)S(1)} %maximum_bitcast_fusion), channel_id=2, replica_groups=mesh['ep'=32,'y2'=2,'y1'=2,'y0'=2,'c'=2] {'y2','y1','y0','c'}, dimensions={0}, use_global_device_ids=true | all-gather | bytes 17408 | tf_op jit(solution)/shard_map/all_gather | solution.py:85
  110.0 0.4 fusion.19
  110.4 2.1 %collective-permute-start.1 = (bf16[64,2048]{1,0:T(8,128)(2,1)S(1)}, bf16[64,2048]{1,0:T(8,128)(2,1)S(1)}, u32[]{:S(2)}, u32[]{:S(2)}) collective-permute-start(bf16[64,2048]{1,0:T(8,128)(2,1)S(1)} %fusion.15), channel_id=1, source_target_pairs={{0,1},{1,0},{2,3},{3,2},{4,5},{5,4},{6,7},{7,6},{8,9},{9,8},{10,11... | collective-permute-start | bytes 786440 | tf_op jit(solution)/shard_map/ppermute | solution.py:31
  112.5 0.3 fusion.10
  112.8 0.3 convolution_add_fusion
  113.2 2.3 %collective-permute-start.9 = (bf16[64,2048]{1,0:T(8,128)(2,1)S(1)}, bf16[64,2048]{1,0:T(8,128)(2,1)S(1)}, u32[]{:S(2)}, u32[]{:S(2)}) collective-permute-start(bf16[64,2048]{1,0:T(8,128)(2,1)S(1)} %fusion.16), channel_id=1, source_target_pairs={{0,1},{1,0},{2,3},{3,2},{4,5},{5,4},{6,7},{7,6},{8,9},{9,8},{10,11... | collective-permute-start | bytes 786440 | tf_op jit(solution)/shard_map/ppermute | solution.py:31
  115.5 0.1 fusion.17
  115.6 1.1 collective-permute-done.9
  116.7 0.1 fusion.18
  116.7 0.1 pad_maximum_fusion.1
  116.8 20.7 %all_to_all.20 = bf16[8,2,8,2048]{3,2,1,0:T(8,128)(2,1)S(1)} all-to-all(bf16[8,2,8,2048]{3,2,1,0:T(8,128)(2,1)S(1)} %pad_maximum_fusion.1), channel_id=1, replica_groups=mesh['ep'=32,'y2'=2,'y1'=2,'y0'=2,'c'=2] {'y2','y1','y0'}, dimensions={0} | all-to-all | bytes 1048576 | tf_op jit(solution)/shard_map/all_to_all | solution.py:35
  137.5 0.1 reduce_sum.62
  137.6 17.7 %all_to_all.21.own_ref = bf16[8,2,8,2048]{3,2,1,0:T(8,128)(2,1)S(1)} all-to-all(bf16[8,2,8,2048]{3,2,1,0:T(8,128)(2,1)S(1)} %broadcast_in_dim.2), channel_id=1, replica_groups=mesh['ep'=32,'y2'=2,'y1'=2,'y0'=2,'c'=2] {'y2','y1','y0'}, dimensions={0} | all-to-all | bytes 1048576 | tf_op jit(solution)/shard_map/all_to_all | solution.py:35
  155.3 5.1 %collective-permute-start.10 = (bf16[8,2,8,2048]{3,2,1,0:T(8,128)(2,1)S(1)}, bf16[8,2,8,2048]{3,2,1,0:T(8,128)(2,1)S(1)}, u32[]{:S(2)}, u32[]{:S(2)}) collective-permute-start(bf16[8,2,8,2048]{3,2,1,0:T(8,128)(2,1)S(1)} %all_to_all.21.own_ref), channel_id=1, source_target_pairs={{0,1},{1,0},{2,3},{3,2},{4,5},{5,4},{6,7},{7,6},{8,9},{9,8},{10,11... | collective-permute-start | bytes 1572872 | tf_op jit(solution)/shard_map/ppermute | solution.py:31
  160.3 1.5 collective-permute-done.10.other_ref
  161.9 1.0 placing.1
  (41 shorter events, 0.3 us)
Async XLA Ops:
  0.6 109.3 %copy-start = (bf16[96,2048]{1,0:T(8,128)(2,1)S(1)}, bf16[96,2048]{1,0:T(8,128)(2,1)}, u32[]{:S(2)}) copy-start(bf16[96,2048]{1,0:T(8,128)(2,1)} %param.20) | copy-start | bytes 1179652
  0.6 28.8 %collective-permute-start.3 = (bf16[2048,128]{1,0:T(8,128)(2,1)}, bf16[2048,128]{1,0:T(8,128)(2,1)S(1)}, u32[]{:S(2)}, u32[]{:S(2)}) collective-permute-start(bf16[2048,128]{1,0:T(8,128)(2,1)} %bitcast.134), channel_id=1, source_target_pairs={{0,2},{2,0},{1,3},{3,1},{4,6},{6,4},{5,7},{7,5},{8,10},{10,8},{9,1... | collective-permute-start | bytes 1572872 | tf_op jit(solution)/shard_map/ppermute | solution.py:31
  6.7 14.4 %copy-start.8 = (bf16[1,2048,128]{2,1,0:T(8,128)(2,1)S(1)}, bf16[1,2048,128]{2,1,0:T(8,128)(2,1)}, u32[]{:S(2)}) copy-start(bf16[1,2048,128]{2,1,0:T(8,128)(2,1)} %param.25) | copy-start | bytes 1572868
  6.7 43.2 %all-to-all-start = ((bf16[32,8,2048]{2,1,0:T(8,128)(2,1)}), bf16[32,8,2048]{2,1,0:T(8,128)(2,1)S(1)}, u32[]{:S(2)}, u32[]{:S(2)}) async-start(bf16[32,8,2048]{2,1,0:T(8,128)(2,1)} %bitcast.129), calls=%async_computation | async-start | bytes 2097152 | tf_op jit(solution)/shard_map/all_to_all | solution.py:35
  18.9 7.2 %copy-start.1 = (bf16[1,128,2048]{2,1,0:T(8,128)(2,1)S(1)}, bf16[1,128,2048]{2,1,0:T(8,128)(2,1)}, u32[]{:S(2)}) copy-start(bf16[1,128,2048]{2,1,0:T(8,128)(2,1)} %param.27) | copy-start | bytes 1572868
  18.9 14.2 %collective-permute-start.4 = (bf16[2048,128]{1,0:T(8,128)(2,1)}, bf16[2048,128]{1,0:T(8,128)(2,1)S(1)}, u32[]{:S(2)}, u32[]{:S(2)}) collective-permute-start(bf16[2048,128]{1,0:T(8,128)(2,1)} %bitcast.48), channel_id=1, source_target_pairs={{0,2},{2,0},{1,3},{3,1},{4,6},{6,4},{5,7},{7,5},{8,10},{10,8},{9,1... | collective-permute-start | bytes 1572872 | tf_op jit(solution)/shard_map/ppermute | solution.py:31
  22.3 10.9 %copy-start.4 = (bf16[2048,256]{1,0:T(8,128)(2,1)}, bf16[2048,256]{1,0:T(8,128)(2,1)S(1)}, u32[]{:S(2)}) copy-start(bf16[2048,256]{1,0:T(8,128)(2,1)S(1)} %pad_maximum_fusion.refs_0_) | copy-start | bytes 3145732
  22.3 26.6 %collective-permute-start.2 = (bf16[2048,256]{1,0:T(8,128)(2,1)S(1)}, bf16[2048,256]{1,0:T(8,128)(2,1)S(1)}, u32[]{:S(2)}, u32[]{:S(2)}) collective-permute-start(bf16[2048,256]{1,0:T(8,128)(2,1)S(1)} %pad_maximum_fusion.refs_0_), channel_id=1, source_target_pairs={{0,1},{1,0},{2,3},{3,2},{4,5},{5,4},{6,7},{7,6},{8,9},{9,8},{10,11... | collective-permute-start | bytes 3145736 | tf_op jit(solution)/shard_map/ppermute | solution.py:31
  26.0 15.4 %copy-start.6 = (bf16[128,2048]{1,0:T(8,128)(2,1)S(1)}, bf16[128,2048]{1,0:T(8,128)(2,1)}, u32[]{:S(2)}) copy-start(bf16[128,2048]{1,0:T(8,128)(2,1)} %param.14) | copy-start | bytes 1572868
  26.1 18.3 %collective-permute-start.7 = (bf16[128,2048]{1,0:T(8,128)(2,1)S(1)}, bf16[128,2048]{1,0:T(8,128)(2,1)S(1)}, u32[]{:S(2)}, u32[]{:S(2)}) collective-permute-start(bf16[128,2048]{1,0:T(8,128)(2,1)S(1)} %bitcast.122), channel_id=1, source_target_pairs={{0,2},{2,0},{1,3},{3,1},{4,6},{6,4},{5,7},{7,5},{8,10},{10,8},{9,1... | collective-permute-start | bytes 1572872 | tf_op jit(solution)/shard_map/ppermute | solution.py:31
  33.2 15.7 %copy-start.5 = (bf16[2048,256]{1,0:T(8,128)(2,1)}, bf16[2048,256]{1,0:T(8,128)(2,1)S(1)}, u32[]{:S(2)}) copy-start(bf16[2048,256]{1,0:T(8,128)(2,1)S(1)} %constant_dynamic-update-slice_fusion.refs_2_) | copy-start | bytes 3145732
  33.2 16.7 %collective-permute-start.5 = (bf16[2048,256]{1,0:T(8,128)(2,1)S(1)}, bf16[2048,256]{1,0:T(8,128)(2,1)}, u32[]{:S(2)}, u32[]{:S(2)}) collective-permute-start(bf16[2048,256]{1,0:T(8,128)(2,1)S(1)} %constant_dynamic-update-slice_fusion.refs_2_), channel_id=1, source_target_pairs={{0,1},{1,0},{2,3},{3,2},{4,5},{5,4},{6,7},{7,6},{8,9},{9,8},{10,11... | collective-permute-start | bytes 3145736 | tf_op jit(solution)/shard_map/ppermute | solution.py:31
  39.5 13.9 %collective-permute-start.6 = (bf16[128,2048]{1,0:T(8,128)(2,1)S(1)}, bf16[128,2048]{1,0:T(8,128)(2,1)S(1)}, u32[]{:S(2)}, u32[]{:S(2)}) collective-permute-start(bf16[128,2048]{1,0:T(8,128)(2,1)S(1)} %bitcast.123), channel_id=1, source_target_pairs={{0,1},{1,0},{2,3},{3,2},{4,5},{5,4},{6,7},{7,6},{8,9},{9,8},{10,11... | collective-permute-start | bytes 1572872 | tf_op jit(solution)/shard_map/ppermute | solution.py:31
  44.3 9.1 %collective-permute-start.8 = (bf16[128,2048]{1,0:T(8,128)(2,1)S(1)}, bf16[128,2048]{1,0:T(8,128)(2,1)}, u32[]{:S(2)}, u32[]{:S(2)}) collective-permute-start(bf16[128,2048]{1,0:T(8,128)(2,1)S(1)} %collective-permute-done.7.refs_2_), channel_id=1, source_target_pairs={{0,1},{1,0},{2,3},{3,2},{4,5},{5,4},{6,7},{7,6},{8,9},{9,8},{10,11... | collective-permute-start | bytes 1572872 | tf_op jit(solution)/shard_map/ppermute | solution.py:31
  48.9 1.0 copy-start.7
  56.0 9.4 %copy-start.11 = (bf16[2048,96]{0,1:T(8,128)(2,1)S(1)}, bf16[2048,96]{0,1:T(8,128)(2,1)}, u32[]{:S(2)}) copy-start(bf16[2048,96]{0,1:T(8,128)(2,1)} %param.16) | copy-start | bytes 1179652
  56.0 9.4 %copy-start.13 = (f32[2048]{0:T(1024)S(1)}, f32[2048]{0:T(1024)}, u32[]{:S(2)}) copy-start(f32[2048]{0:T(1024)} %param.15) | copy-start | bytes 24580
  56.0 56.5 %all-to-all-start.1 = ((bf16[32,8,2048]{2,1,0:T(8,128)(2,1)}), bf16[32,8,2048]{2,1,0:T(8,128)(2,1)S(1)}, u32[]{:S(2)}, u32[]{:S(2)}) async-start(bf16[32,8,2048]{2,1,0:T(8,128)(2,1)} %bitcast.128), calls=%async_computation.1 | async-start | bytes 2097152 | tf_op jit(solution)/shard_map/all_to_all | solution.py:35
  65.4 1.0 copy-start.12
  66.4 3.6 %copy-start.9 = (f32[31,96]{1,0:T(8,128)S(1)}, f32[31,96]{1,0:T(8,128)}, u32[]{:S(2)}) copy-start(f32[31,96]{1,0:T(8,128)} %param.18) | copy-start | bytes 35716
  66.4 3.6 %copy-start.2 = (s32[128,4]{0,1:T(4,128)S(1)}, s32[128,4]{0,1:T(4,128)}, u32[]{:S(2)}) copy-start(s32[128,4]{0,1:T(4,128)} %param.23) | copy-start | bytes 6148
  66.4 3.7 %copy-start.3 = (f32[128,4]{0,1:T(4,128)S(1)}, f32[128,4]{0,1:T(4,128)}, u32[]{:S(2)}) copy-start(f32[128,4]{0,1:T(4,128)} %param.24) | copy-start | bytes 6148
  66.4 43.6 %copy-start.10 = (f32[96]{0:T(128)S(1)}, f32[96]{0:T(128)}, u32[]{:S(2)}) copy-start(f32[96]{0:T(128)} %param.19) | copy-start | bytes 1156
  66.9 23.2 %collective-permute-start = (bf16[30,96]{0,1:T(8,128)(2,1)S(1)}, bf16[30,96]{0,1:T(8,128)(2,1)S(1)}, u32[]{:S(2)}, u32[]{:S(2)}) collective-permute-start(bf16[30,96]{0,1:T(8,128)(2,1)S(1)} %slice.256), channel_id=1, source_target_pairs={{0,16},{16,32},{32,48},{48,64},{64,80},{80,96},{96,112},{112,128},... | collective-permute-start | bytes 17288 | tf_op jit(solution)/shard_map/ppermute | solution.py:27
  110.4 5.1 %collective-permute-start.1 = (bf16[64,2048]{1,0:T(8,128)(2,1)S(1)}, bf16[64,2048]{1,0:T(8,128)(2,1)S(1)}, u32[]{:S(2)}, u32[]{:S(2)}) collective-permute-start(bf16[64,2048]{1,0:T(8,128)(2,1)S(1)} %fusion.15), channel_id=1, source_target_pairs={{0,1},{1,0},{2,3},{3,2},{4,5},{5,4},{6,7},{7,6},{8,9},{9,8},{10,11... | collective-permute-start | bytes 786440 | tf_op jit(solution)/shard_map/ppermute | solution.py:31
  113.2 3.4 %collective-permute-start.9 = (bf16[64,2048]{1,0:T(8,128)(2,1)S(1)}, bf16[64,2048]{1,0:T(8,128)(2,1)S(1)}, u32[]{:S(2)}, u32[]{:S(2)}) collective-permute-start(bf16[64,2048]{1,0:T(8,128)(2,1)S(1)} %fusion.16), channel_id=1, source_target_pairs={{0,1},{1,0},{2,3},{3,2},{4,5},{5,4},{6,7},{7,6},{8,9},{9,8},{10,11... | collective-permute-start | bytes 786440 | tf_op jit(solution)/shard_map/ppermute | solution.py:31
  155.3 6.6 %collective-permute-start.10 = (bf16[8,2,8,2048]{3,2,1,0:T(8,128)(2,1)S(1)}, bf16[8,2,8,2048]{3,2,1,0:T(8,128)(2,1)S(1)}, u32[]{:S(2)}, u32[]{:S(2)}) collective-permute-start(bf16[8,2,8,2048]{3,2,1,0:T(8,128)(2,1)S(1)} %all_to_all.21.own_ref), channel_id=1, source_target_pairs={{0,1},{1,0},{2,3},{3,2},{4,5},{5,4},{6,7},{7,6},{8,9},{9,8},{10,11... | collective-permute-start | bytes 1572872 | tf_op jit(solution)/shard_map/ppermute | solution.py:31
